TPU v7x, 32 devices: a whole 2x2x4 slice. The times are simulated.
32 devices in a mesh: rep: 2 (over x), fs: 8 (over z, y), tp: 2 (over core).
Axes of the slice: x: 2, y: 2, z: 4, core: 2. Of those that a mesh axis runs over, the one named last changes fastest.
Arguments:
- tokens: bfloat16 [8192, 2048], P(('rep', 'fs')), may hold values from -3 to 3
- mixer_gain: float32 [2048], replicated, may hold values from 0.1 to 1.9
- mix_weight: bfloat16 [2048, 1024], P('fs', 'tp'), may hold values from -0.125 to 0.125
- mixer_conv: float32 [4, 1024], P(None, 'tp'), may hold values from -3 to 3
- mixer_offset: float32 [1024], P('tp'), may hold values from -0.06 to 0.06
- recur_weight: bfloat16 [8, 128, 128], P('tp'), may hold values from -0.5 to 0.5
- recur_bias: float32 [1024], P('tp'), may hold values from -3 to 3
- input_weight: bfloat16 [8, 128, 128], P('tp'), may hold values from -0.5 to 0.5
- input_bias: float32 [1024], P('tp'), may hold values from 1 to 3
- decay_logit: float32 [1024], P('tp'), may hold values from 4 to 11
- out_weight: bfloat16 [1024, 2048], P('tp', 'fs'), may hold values from -0.375 to 0.375
- channel_gain: float32 [2048], replicated, may hold values from 0.1 to 1.9
- gate_weight: bfloat16 [2048, 6144], P('fs', 'tp'), may hold values from -0.125 to 0.125
- up_weight: bfloat16 [2048, 6144], P('fs', 'tp'), may hold values from -0.125 to 0.125
- gate_conv: float32 [3, 6144], P(None, 'tp'), may hold values from -3.5 to 3.5
- gate_offset: float32 [6144], P('tp'), may hold values from -3 to 3
- down_weight: bfloat16 [6144, 2048], P('tp', 'fs'), may hold values from -0.078125 to 0.078125
Outputs:
- layer_out: bfloat16 [8192, 2048], P(('rep', 'fs'))
All inputs are finite; a program needn't handle non-finite values.
Results may differ from a plain program's by a relative error of at most 0.023.
Values may be sent and summed in bfloat16 or wider, within the bound.
A program may use at most 128 MiB of HBM per device.

v0:
```python
import functools

import jax
import jax.numpy as jnp
from jax import lax
from jax.experimental import pallas as pl
from jax.experimental.pallas import tpu as pltpu
from jax.sharding import PartitionSpec as P

epsilon = 1e-06
lru_scale = 8.0


def rms_rows(values, gain_row):
    widened = values.astype(jnp.float32)
    scaled = widened * lax.rsqrt(jnp.mean(widened * widened, axis=-1, keepdims=True) + epsilon)
    return (scaled * gain_row).astype(jnp.bfloat16)


def causal_conv(values, tap_rows, offset):
    width = tap_rows.shape[0]
    length = values.shape[-2]
    padding = [(0, 0)] * (values.ndim - 2) + [(width - 1, 0), (0, 0)]
    padded = jnp.pad(values, padding)
    total = offset + padded[..., 0:length, :] * tap_rows[0]
    for tap_index in range(1, width):
        total = total + padded[..., tap_index : tap_index + length, :] * tap_rows[tap_index]
    return total


def one_minus_exp(v):
    series = 1.0 + v * (1.0 / 7.0)
    for order in (6.0, 5.0, 4.0, 3.0, 2.0):
        series = 1.0 + v * (1.0 / order) * series
    return jnp.where(v > -0.25, -v * series, 1.0 - jnp.exp(v))


def mixer_kernel(
    branch_ref, taps_ref, offset_ref, recur_ref, recur_bias_ref, input_ref, input_bias_ref, rate_ref, out_ref
):
    branch = branch_ref[...].astype(jnp.float32)
    length = branch.shape[0]
    width = taps_ref.shape[0]
    rows = lax.broadcasted_iota(jnp.int32, branch.shape, 0)

    def shifted(values, step, fill):
        return jnp.where(rows >= step, pltpu.roll(values, step, 0), fill)

    total = offset_ref[...] + branch * taps_ref[width - 1 : width, :]
    for back in range(1, width):
        total = total + shifted(branch, back, 0.0) * taps_ref[width - 1 - back : width - back, :]
    smoothed = total.astype(jnp.bfloat16)
    recur = jnp.dot(smoothed, recur_ref[0], preferred_element_type=jnp.float32)
    recur_gate = jax.nn.sigmoid(recur + recur_bias_ref[...])
    gated = jnp.dot(smoothed, input_ref[0], preferred_element_type=jnp.float32)
    input_gate = jax.nn.sigmoid(gated + input_bias_ref[...])
    log_decay = recur_gate * rate_ref[...]
    state = jnp.sqrt(one_minus_exp(2.0 * log_decay)) * (input_gate * smoothed.astype(jnp.float32))
    decay = jnp.exp(log_decay)
    step = 1
    while step < length:
        state = state + decay * shifted(state, step, 0.0)
        if 2 * step < length:
            decay = decay * shifted(decay, step, 1.0)
        step *= 2
    out_ref[...] = state.astype(jnp.bfloat16)


def mixer(branch, taps, offset, recur_weight, recur_bias, input_weight, input_bias, rate):
    length, channels = branch.shape
    blocks, dim, _ = recur_weight.shape
    column = lambda rows: pl.BlockSpec((rows, dim), lambda k: (0, k))
    square = pl.BlockSpec((1, dim, dim), lambda k: (k, 0, 0))
    row = lambda v: v.reshape(1, channels)
    return pl.pallas_call(
        mixer_kernel,
        name="mixer",
        grid=(blocks,),
        in_specs=[
            column(length),
            column(taps.shape[0]),
            column(1),
            square,
            column(1),
            square,
            column(1),
            column(1),
        ],
        out_specs=column(length),
        out_shape=jax.ShapeDtypeStruct((length, channels), jnp.bfloat16),
        cost_estimate=pl.CostEstimate(
            flops=60 * length * channels + 4 * length * channels * dim,
            bytes_accessed=4 * length * channels,
            transcendentals=5 * length * channels,
        ),
    )(
        branch,
        taps,
        row(offset),
        recur_weight,
        row(recur_bias),
        input_weight,
        row(input_bias),
        row(rate),
    )


def shift(values, axis, count, step):
    return lax.ppermute(values, axis, [(i, (i + step) % count) for i in range(count)])


def take(values, index, size, axis=0):
    return lax.dynamic_slice_in_dim(values, index * size, size, axis)


def pair_gather(weight, count, axis):
    groups = [list(range(parity, count, 2)) for parity in range(2)]
    own = lax.all_gather(weight, "fs", axis=axis, axis_index_groups=groups, tiled=True)
    other = lax.ppermute(own, "fs", [(i, i ^ 1) for i in range(count)])
    return own, other


def pair_columns(values, count, parity):
    rows, width = values.shape
    size = width // count
    blocks = [values[:, i * size : (i + 1) * size] for i in range(count)]
    even = jnp.concatenate(blocks[0::2], axis=1)
    odd = jnp.concatenate(blocks[1::2], axis=1)
    return jnp.where(parity == 0, even, odd), jnp.where(parity == 0, odd, even)


def scatter_rows(partial, n_tp, me):
    size = partial.shape[0] // n_tp
    total = take(partial, me, size).astype(jnp.float32)
    for step in range(1, n_tp):
        sent = take(partial, lax.rem(me + step, n_tp), size)
        total = total + shift(sent, "tp", n_tp, step).astype(jnp.float32)
    return total


def collect_rows(share, n_tp, me):
    size = share.shape[0]
    if n_tp == 2:
        other = shift(share, "tp", n_tp, 1)
        first = jnp.where(me == 0, share, other)
        second = jnp.where(me == 0, other, share)
        return jnp.concatenate([first, second], axis=0)
    whole = jnp.zeros((size * n_tp, share.shape[1]), share.dtype)
    whole = lax.dynamic_update_slice_in_dim(whole, share, me * size, 0)
    for step in range(1, n_tp):
        got = shift(share, "tp", n_tp, step)
        whole = lax.dynamic_update_slice_in_dim(whole, got, lax.rem(me - step + n_tp, n_tp) * size, 0)
    return whole


def local(
    n_rep,
    n_fs,
    n_tp,
    tokens,
    mixer_gain,
    mix_weight,
    mixer_conv,
    mixer_offset,
    recur_weight,
    recur_bias,
    input_weight,
    input_bias,
    decay_logit,
    out_weight,
    channel_gain,
    gate_weight,
    up_weight,
    gate_conv,
    gate_offset,
    down_weight,
):
    rep = lax.axis_index("rep")
    tp = lax.axis_index("tp")
    parity = lax.rem(lax.axis_index("fs"), 2)
    length = tokens.shape[0]
    units = gate_weight.shape[1] // n_rep

    both = jnp.concatenate([mix_weight, out_weight.T], axis=1)
    both_full = lax.all_gather(both, "fs", axis=0, tiled=True)
    channels = mix_weight.shape[1]
    mixer_full, out_full = both_full[:, :channels], both_full[:, channels:]
    gate_own, gate_other = pair_gather(take(gate_weight, rep, units, 1), n_fs, 0)
    up_own, up_other = pair_gather(take(up_weight, rep, units, 1), n_fs, 0)
    down_full = lax.all_gather(take(down_weight, rep, units, 0), "fs", axis=1, tiled=True)
    gate_taps = take(gate_conv, rep, units, 1)
    gate_base = take(gate_offset, rep, units, 0)

    normed = rms_rows(tokens, mixer_gain)
    branch = jnp.dot(normed, mixer_full, preferred_element_type=jnp.float32).astype(jnp.bfloat16)
    recurrent = mixer(
        branch,
        mixer_conv,
        mixer_offset,
        recur_weight,
        recur_bias,
        input_weight,
        input_bias,
        lru_scale * jax.nn.log_sigmoid(decay_logit),
    )
    mixer_term = lax.dot_general(
        recurrent, out_full, (((1,), (1,)), ((), ())), preferred_element_type=jnp.float32
    )
    mixer_share = scatter_rows(mixer_term.astype(jnp.bfloat16), n_tp, tp)
    rows = length // n_tp
    residual = (take(tokens, tp, rows).astype(jnp.float32) + mixer_share).astype(jnp.bfloat16)
    normed_share = rms_rows(residual, channel_gain)

    shares = [normed_share]
    for step in range(1, n_rep):
        shares.append(shift(normed_share, "rep", n_rep, step))

    def channel_mixer(share):
        rows_in = collect_rows(share, n_tp, tp)
        left, right = pair_columns(rows_in, n_fs, parity)
        gate_rows = jnp.dot(left, gate_own, preferred_element_type=jnp.float32)
        gate_rows = gate_rows + jnp.dot(right, gate_other, preferred_element_type=jnp.float32)
        up_rows = jnp.dot(left, up_own, preferred_element_type=jnp.float32)
        up_rows = up_rows + jnp.dot(right, up_other, preferred_element_type=jnp.float32)
        gate_rows = gate_rows.astype(jnp.bfloat16)
        up_rows = up_rows.astype(jnp.bfloat16)
        gate_mixed = causal_conv(gate_rows.astype(jnp.float32), gate_taps, gate_base)
        hidden = (jax.nn.gelu(gate_mixed) * up_rows.astype(jnp.float32)).astype(jnp.bfloat16)
        return jnp.dot(hidden, down_full, preferred_element_type=jnp.float32).astype(jnp.bfloat16)

    own_terms = channel_mixer(shares[0])
    total = None
    for step in range(1, n_rep):
        summed = scatter_rows(channel_mixer(shares[step]), n_tp, tp).astype(jnp.bfloat16)
        back = shift(summed, "rep", n_rep, -step).astype(jnp.float32)
        total = back if total is None else total + back
    own = scatter_rows(own_terms, n_tp, tp)
    total = own if total is None else own + total
    result = (residual.astype(jnp.float32) + total).astype(jnp.bfloat16)
    return collect_rows(result, n_tp, tp)


def solution(mesh):
    in_specs = (
        P(("rep", "fs"), None),
        P(),
        P("fs", "tp"),
        P(None, "tp"),
        P("tp"),
        P("tp", None, None),
        P("tp"),
        P("tp", None, None),
        P("tp"),
        P("tp"),
        P("tp", "fs"),
        P(),
        P("fs", "tp"),
        P("fs", "tp"),
        P(None, "tp"),
        P("tp"),
        P("tp", "fs"),
    )
    out_specs = P(("rep", "fs"), None)
    body = functools.partial(local, mesh.shape["rep"], mesh.shape["fs"], mesh.shape["tp"])
    return jax.shard_map(body, mesh=mesh, in_specs=in_specs, out_specs=out_specs, check_vma=False)
```

profile of v0, /device:TPU:0, one launch (start us, length us, event | category | flops | bytes accessed | tf_op | source)
XLA Modules:
  0.0 421.8 jit_solution(7286322764803237131)
XLA Ops:
  7.7 1.8 pad_maximum_fusion.3
  10.7 2.2 constant_dynamic-slice_fusion.3
  13.0 2.1 constant_dynamic-slice_fusion.2
  16.3 70.8 %all-gather.5.cloned.1.call-done = bf16[2048,1024]{0,1:T(8,128)(2,1)} async-done(((bf16[256,1024]{0,1:T(8,128)(2,1)}), bf16[2048,1024]{0,1:T(8,128)(2,1)}) %all-gather.5.cloned.1.call-update) | async-done | bytes 4194320 | tf_op jit(solution)/shard_map/all_gather | solution.py:185
  87.1 3.7 fusion.41.branch_ref
  90.8 5.6 %mixer.1 = bf16[512,512]{1,0:T(8,128)(2,1)} custom-call(bf16[512,512]{1,0:T(8,128)(2,1)} %fusion.41.branch_ref, f32[4,512]{1,0:T(4,128)} %taps_ref.1, f32[1,512]{1,0:T(1,128)} %bitcast.18, bf16[4,128,128]{2,1,0:T(8,128)(2,1)} %recur_ref.1, f32[1,512]{1,0:T(1,128)} %bitcast.19, bf16[4,128,128]{2,1,0:T(8,128)(2,1)} %input_ref.1, f32[1,512]{1,0:T(1,128)} %bitcast.20, ...), custom_call_target="tpu_custom_call" | custom-call | flops 149946368 | bytes 1048576 | tf_op jit(solution)/shard_map/mixer/pallas_call | solution.py:75
  96.4 4.3 %convolution_convert_fusion.2 = bf16[512,2048]{1,0:T(8,128)(2,1)} fusion(bf16[512,512]{1,0:T(8,128)(2,1)} %mixer.1, bf16[2048,1024]{0,1:T(8,128)(2,1)} %all-gather.5.cloned.1.call-done), kind=kOutput, calls=%fused_computation.68 | convolution fusion | flops 1074790400 | bytes 4718592 | tf_op jit(solution)/shard_map/dot_general | solution.py:206
  100.7 1.3 constant_dynamic-slice_fusion.5
  102.1 48.2 %all-gather.7.cloned.1.call-done = bf16[1024,1536]{1,0:T(8,128)(2,1)} async-done(((bf16[256,1536]{1,0:T(8,128)(2,1)}), bf16[1024,1536]{1,0:T(8,128)(2,1)}) %all-gather.7.cloned.1.call-update) | async-done | bytes 3145744 | tf_op jit(solution)/shard_map/all_gather | solution.py:118
  150.3 1.5 collective-permute-start.2
  151.8 2.2 fusion.27
  154.0 1.3 fusion.29
  155.3 1.5 collective-permute-start.5
  157.8 56.2 %all-gather.9.cloned.1.call-done = bf16[1024,1536]{1,0:T(8,128)(2,1)} async-done(((bf16[256,1536]{1,0:T(8,128)(2,1)}), bf16[1024,1536]{1,0:T(8,128)(2,1)}) %all-gather.9.cloned.1.call-update) | async-done | bytes 3145744 | tf_op jit(solution)/shard_map/all_gather | solution.py:118
  214.0 1.5 collective-permute-start.3
  216.5 2.4 copy-done.17
  218.9 3.4 fusion.50
  222.3 1.8 fusion.51
  224.2 5.4 %fusion.22 = f32[512,1536]{1,0:T(8,128)} fusion(f32[512,1536]{1,0:T(8,128)S(1)} %fusion.51, bf16[1024,1536]{1,0:T(8,128)(2,1)} %collective-permute-done.2, bf16[512,1024]{1,0:T(8,128)(2,1)S(1)} %fusion.47, pred[]{:T(512)S(6)} %eq.5, bf16[512,256]{1,0:T(8,128)(2,1)S(1)} %get-tuple-element.15, bf16[512,256]{1,0:T(8,128)(2,1)S(1)} %get-tuple-element.14, ...), kind=kOutput, calls=%fused_computation.61 | convolution fusion | flops 1617690624 | bytes 11534337 | tf_op jit(solution)/shard_map/dot_general | solution.py:222
  230.2 3.5 fusion.52
  233.8 1.8 fusion.53
  235.6 5.4 %fusion.25 = f32[512,1536]{1,0:T(8,128)} fusion(f32[512,1536]{1,0:T(8,128)S(1)} %fusion.53, bf16[1024,1536]{1,0:T(8,128)(2,1)} %collective-permute-done.2, bf16[512,1024]{1,0:T(8,128)(2,1)S(1)} %fusion.49, pred[]{:T(512)S(6)} %eq.5, bf16[512,256]{1,0:T(8,128)(2,1)S(1)} %get-tuple-element.24, bf16[512,256]{1,0:T(8,128)(2,1)S(1)} %get-tuple-element.23, ...), kind=kOutput, calls=%fused_computation.64 | convolution fusion | flops 1617690624 | bytes 11534337 | tf_op jit(solution)/shard_map/dot_general | solution.py:222
  241.1 83.9 %collective-permute-done.3 = bf16[1024,1536]{1,0:T(8,128)(2,1)} collective-permute-done((bf16[1024,1536]{1,0:T(8,128)(2,1)}, bf16[1024,1536]{1,0:T(8,128)(2,1)}, u32[]{:S(2)}, u32[]{:S(2)}) %collective-permute-start.3) | collective-permute-done | bytes 3145760 | tf_op jit(solution)/shard_map/ppermute | solution.py:119
  325.0 24.1 %all-gather.11.cloned.1.call-done = bf16[1536,2048]{1,0:T(8,128)(2,1)} async-done(((bf16[1536,256]{1,0:T(8,128)(2,1)}), bf16[1536,2048]{1,0:T(8,128)(2,1)}) %all-gather.11.cloned.1.call-update) | async-done | bytes 6291472 | tf_op jit(solution)/shard_map/all_gather | solution.py:190
  349.2 15.0 %convolution_convert_fusion = bf16[512,2048]{1,0:T(8,128)(2,1)S(1)} fusion(bf16[1536,2048]{1,0:T(8,128)(2,1)} %all-gather.11.cloned.1.call-done, f32[512,1536]{1,0:T(8,128)} %fusion.25, f32[512,1536]{1,0:T(8,128)} %fusion.52, bf16[1024,1536]{1,0:T(8,128)(2,1)} %collective-permute-done.3, f32[1536]{0:T(1024)S(1)} %get-tuple-element.7, ...), kind=kOutput, calls=%fused_computation.66 | convolution fusion | flops 4852547584 | bytes 19947520 | tf_op jit(solution)/shard_map/dot_general | solution.py:229
  365.2 15.8 %convolution_convert_fusion.1 = bf16[512,2048]{1,0:T(8,128)(2,1)} fusion(bf16[1536,2048]{1,0:T(8,128)(2,1)} %all-gather.11.cloned.1.call-done, f32[512,1536]{1,0:T(8,128)} %fusion.22, f32[512,1536]{1,0:T(8,128)} %fusion.50, bf16[1024,1536]{1,0:T(8,128)(2,1)} %collective-permute-done.3, f32[1536]{0:T(1024)S(1)} %get-tuple-element.7, ...), kind=kOutput, calls=%fused_computation.67 | convolution fusion | flops 4852547584 | bytes 19947520 | tf_op jit(solution)/shard_map/dot_general | solution.py:229
  381.0 1.3 constant_dynamic-slice_fusion.1
  382.9 1.7 add_convert_fusion
  384.5 1.5 collective-permute-start.8
  386.1 23.7 %collective-permute-done.8 = bf16[256,2048]{1,0:T(8,128)(2,1)S(1)} collective-permute-done((bf16[256,2048]{1,0:T(8,128)(2,1)S(1)}, bf16[256,2048]{1,0:T(8,128)(2,1)S(1)}, u32[]{:S(2)}, u32[]{:S(2)}) %collective-permute-start.8) | collective-permute-done | bytes 1048608 | tf_op jit(solution)/shard_map/ppermute | solution.py:109
  410.6 2.6 collective-permute-done.9
  413.4 1.6 pad_maximum_fusion
  (75 shorter events, 9.0 us)
Async XLA Ops:
  6.5 3.1 copy-start
  6.5 80.5 %all-gather.5.cloned.1.call-start = ((), (), s32[]{:S(2)}) async-start(), calls=%async_computation | async-start | bytes 4718592 | tf_op jit(solution)/shard_map/all_gather | solution.py:185
  9.6 140.7 %all-gather.7.cloned.1.call-start = ((), (), s32[]{:S(2)}) async-start(), calls=%async_computation.1 | async-start | bytes 3932160 | tf_op jit(solution)/shard_map/all_gather | solution.py:118
  10.6 4.5 %copy-start.2 = (bf16[512,2048]{1,0:T(8,128)(2,1)S(1)}, bf16[512,2048]{1,0:T(8,128)(2,1)}, u32[]{:S(2)}) copy-start(bf16[512,2048]{1,0:T(8,128)(2,1)} %param.17) | copy-start | bytes 6291460
  10.6 203.4 %all-gather.9.cloned.1.call-start = ((), (), s32[]{:S(2)}) async-start(), calls=%async_computation.2 | async-start | bytes 3932160 | tf_op jit(solution)/shard_map/all_gather | solution.py:118
  12.9 2.7 copy-start.15
  12.9 74.1 %copy-start.18 = (f32[2048]{0:T(1024)S(1)}, f32[2048]{0:T(1024)}, u32[]{:S(2)}) copy-start(f32[2048]{0:T(1024)} %param.18) | copy-start | bytes 24580
  13.0 336.2 %all-gather.11.cloned.1.call-start = ((), (), s32[]{:S(2)}) async-start(), calls=%async_computation.3 | async-start | bytes 7077888 | tf_op jit(solution)/shard_map/all_gather | solution.py:190
  102.0 49.7 %collective-permute-start = (bf16[256,2048]{1,0:T(8,128)(2,1)S(1)}, bf16[256,2048]{1,0:T(8,128)(2,1)}, u32[]{:S(2)}, u32[]{:S(2)}) collective-permute-start(bf16[256,2048]{1,0:T(8,128)(2,1)S(1)} %constant_dynamic-slice_fusion.5), channel_id=1, source_target_pairs={{0,1},{1,0},{2,3},{3,2},{4,5},{5,4},{6,7},{7,6},{8,9},{9,8},{10,11... | collective-permute-start | bytes 3145736 | tf_op jit(solution)/shard_map/ppermute | solution.py:109
  102.1 51.9 %copy-start.13 = (f32[2048]{0:T(1024)S(1)}, f32[2048]{0:T(1024)}, u32[]{:S(2)}) copy-start(f32[2048]{0:T(1024)} %param.28) | copy-start | bytes 24580
  150.3 73.9 %collective-permute-start.2 = (bf16[1024,1536]{1,0:T(8,128)(2,1)}, bf16[1024,1536]{1,0:T(8,128)(2,1)}, u32[]{:S(2)}, u32[]{:S(2)}) collective-permute-start(bf16[1024,1536]{1,0:T(8,128)(2,1)} %all-gather.7.cloned.1.call-done), channel_id=1, source_target_pairs={{0,2},{2,0},{4,6},{6,4},{8,10},{10,8},{12,14},{14,12},{1,3},{3,1},... | collective-permute-start | bytes 9437192 | tf_op jit(solution)/shard_map/ppermute | solution.py:119
  153.9 2.8 copy-start.14
  155.3 60.2 %collective-permute-start.5 = (bf16[256,2048]{1,0:T(8,128)(2,1)}, bf16[256,2048]{1,0:T(8,128)(2,1)S(1)}, u32[]{:S(2)}, u32[]{:S(2)}) collective-permute-start(bf16[256,2048]{1,0:T(8,128)(2,1)} %fusion.29), channel_id=1, source_target_pairs={{0,16},{16,0},{1,17},{17,1},{2,18},{18,2},{3,19},{19,3},{4,20},{20... | collective-permute-start | bytes 3145736 | tf_op jit(solution)/shard_map/ppermute | solution.py:109
  156.7 58.7 %collective-permute-start.1 = (bf16[256,2048]{1,0:T(8,128)(2,1)}, bf16[256,2048]{1,0:T(8,128)(2,1)S(1)}, u32[]{:S(2)}, u32[]{:S(2)}) collective-permute-start(bf16[256,2048]{1,0:T(8,128)(2,1)} %fusion.29), channel_id=1, source_target_pairs={{0,1},{1,0},{2,3},{3,2},{4,5},{5,4},{6,7},{7,6},{8,9},{9,8},{10,11... | collective-permute-start | bytes 3145736 | tf_op jit(solution)/shard_map/ppermute | solution.py:109
  214.0 111.0 %collective-permute-start.3 = (bf16[1024,1536]{1,0:T(8,128)(2,1)}, bf16[1024,1536]{1,0:T(8,128)(2,1)}, u32[]{:S(2)}, u32[]{:S(2)}) collective-permute-start(bf16[1024,1536]{1,0:T(8,128)(2,1)} %all-gather.9.cloned.1.call-done), channel_id=1, source_target_pairs={{0,2},{2,0},{4,6},{6,4},{8,10},{10,8},{12,14},{14,12},{1,3},{3,1},... | collective-permute-start | bytes 9437192 | tf_op jit(solution)/shard_map/ppermute | solution.py:119
  215.5 14.2 %collective-permute-start.6 = (bf16[256,2048]{1,0:T(8,128)(2,1)S(1)}, bf16[256,2048]{1,0:T(8,128)(2,1)S(1)}, u32[]{:S(2)}, u32[]{:S(2)}) collective-permute-start(bf16[256,2048]{1,0:T(8,128)(2,1)S(1)} %collective-permute-done.5), channel_id=1, source_target_pairs={{0,1},{1,0},{2,3},{3,2},{4,5},{5,4},{6,7},{7,6},{8,9},{9,8},{10,11... | collective-permute-start | bytes 3145736 | tf_op jit(solution)/shard_map/ppermute | solution.py:109
  216.3 7.9 %copy-start.6 = (bf16[512,256]{1,0:T(8,128)(2,1)}, bf16[512,256]{1,0:T(8,128)(2,1)S(1)}, u32[]{:S(2)}) copy-start(bf16[512,256]{1,0:T(8,128)(2,1)S(1)} %get-tuple-element.13) | copy-start | bytes 786436
  216.3 7.9 %copy-start.7 = (bf16[512,256]{1,0:T(8,128)(2,1)}, bf16[512,256]{1,0:T(8,128)(2,1)S(1)}, u32[]{:S(2)}) copy-start(bf16[512,256]{1,0:T(8,128)(2,1)S(1)} %get-tuple-element.14) | copy-start | bytes 786436
  216.3 7.9 %copy-start.8 = (bf16[512,256]{1,0:T(8,128)(2,1)}, bf16[512,256]{1,0:T(8,128)(2,1)S(1)}, u32[]{:S(2)}) copy-start(bf16[512,256]{1,0:T(8,128)(2,1)S(1)} %get-tuple-element.15) | copy-start | bytes 786436
  216.3 2.5 copy-start.17
  216.5 7.7 %copy-start.4 = (bf16[512,1024]{1,0:T(8,128)(2,1)}, bf16[512,1024]{1,0:T(8,128)(2,1)S(1)}, u32[]{:S(2)}) copy-start(bf16[512,1024]{1,0:T(8,128)(2,1)S(1)} %fusion.47) | copy-start | bytes 3145732
  218.9 3.5 copy-start.16
  230.0 5.5 %copy-start.9 = (bf16[512,256]{1,0:T(8,128)(2,1)}, bf16[512,256]{1,0:T(8,128)(2,1)S(1)}, u32[]{:S(2)}) copy-start(bf16[512,256]{1,0:T(8,128)(2,1)S(1)} %get-tuple-element.21) | copy-start | bytes 786436
  230.1 5.5 %copy-start.10 = (bf16[512,256]{1,0:T(8,128)(2,1)}, bf16[512,256]{1,0:T(8,128)(2,1)S(1)}, u32[]{:S(2)}) copy-start(bf16[512,256]{1,0:T(8,128)(2,1)S(1)} %get-tuple-element.22) | copy-start | bytes 786436
  230.1 5.5 %copy-start.11 = (bf16[512,256]{1,0:T(8,128)(2,1)}, bf16[512,256]{1,0:T(8,128)(2,1)S(1)}, u32[]{:S(2)}) copy-start(bf16[512,256]{1,0:T(8,128)(2,1)S(1)} %get-tuple-element.23) | copy-start | bytes 786436
  230.1 5.5 %copy-start.12 = (bf16[512,256]{1,0:T(8,128)(2,1)}, bf16[512,256]{1,0:T(8,128)(2,1)S(1)}, u32[]{:S(2)}) copy-start(bf16[512,256]{1,0:T(8,128)(2,1)S(1)} %get-tuple-element.24) | copy-start | bytes 786436
  230.2 5.4 %copy-start.5 = (bf16[512,1024]{1,0:T(8,128)(2,1)}, bf16[512,1024]{1,0:T(8,128)(2,1)S(1)}, u32[]{:S(2)}) copy-start(bf16[512,1024]{1,0:T(8,128)(2,1)S(1)} %fusion.49) | copy-start | bytes 3145732
  365.2 17.7 %collective-permute-start.7 = (bf16[256,2048]{1,0:T(8,128)(2,1)}, bf16[256,2048]{1,0:T(8,128)(2,1)}, u32[]{:S(2)}, u32[]{:S(2)}) collective-permute-start(bf16[256,2048]{1,0:T(8,128)(2,1)} %constant_dynamic-slice_fusion), channel_id=1, source_target_pairs={{0,1},{1,0},{2,3},{3,2},{4,5},{5,4},{6,7},{7,6},{8,9},{9,8},{10,11... | collective-permute-start | bytes 3145736 | tf_op jit(solution)/shard_map/ppermute | solution.py:109
  382.3 27.5 %copy-start.3 = (bf16[512,2048]{1,0:T(8,128)(2,1)S(1)}, bf16[512,2048]{1,0:T(8,128)(2,1)}, u32[]{:S(2)}) copy-start(bf16[512,2048]{1,0:T(8,128)(2,1)} %convolution_convert_fusion.1) | copy-start | bytes 6291460
  382.3 3.8 collective-permute-start.4
  384.5 25.2 %collective-permute-start.8 = (bf16[256,2048]{1,0:T(8,128)(2,1)S(1)}, bf16[256,2048]{1,0:T(8,128)(2,1)S(1)}, u32[]{:S(2)}, u32[]{:S(2)}) collective-permute-start(bf16[256,2048]{1,0:T(8,128)(2,1)S(1)} %add_convert_fusion), channel_id=1, source_target_pairs={{0,16},{16,0},{1,17},{17,1},{2,18},{18,2},{3,19},{19,3},{4,20},{20... | collective-permute-start | bytes 3145736 | tf_op jit(solution)/shard_map/ppermute | solution.py:109
  410.5 2.7 collective-permute-start.9
  (1 other events, 1.9 us)
Sparse Core Ops, SparseCore 0:
  9.7 77.3 all-gather.4
  88.6 61.6 all-gather.6
  151.9 62.0 all-gather.8
  215.9 133.2 all-gather.10
where the time goes:
time: 423 us; the launch traced here: 422 us
  waiting for transfers between devices  310 us (73%)
  matrix products  60.3 us (14%)
  local copies, waits for them, and re-layouts  14 us (3%)
  between operations  13.5 us (3%)
  other arithmetic  11.9 us (3%)
  starting transfers between devices  6.79 us (2%)
  Pallas kernels  5.63 us (1%)
    all_gather x2, waiting for transfers between devices, pair_gather(): lax.all_gather(weight, 'fs', axis=axis, axis_index_groups=groups, tiled=T...  104 us
    ppermute x2, waiting for transfers between devices, pair_gather(): other = lax.ppermute(own, 'fs', [(i, i ^ 1) for i in range(count)])  84 us
    all_gather x1, waiting for transfers between devices, local(): both_full = lax.all_gather(both, 'fs', axis=0, tiled=True)  70.8 us
    dot_general x2, matrix products, channel_mixer(): jnp.dot(hidden, down_full, preferred_element_type=jnp.float32)  30.8 us
    ppermute x8, waiting for transfers between devices, shift(): lax.ppermute(values, axis, [(i, (i + step) % count) for i in range(count)])  26.4 us
    all_gather x1, waiting for transfers between devices, local(): lax.all_gather(take(down_weight, rep, units, 0), 'fs', axis=1, tiled=True)  24.1 us
    dot_general x2, matrix products, channel_mixer(): jnp.dot(right, gate_other, preferred_element_type=jnp.float32)  10.9 us
    dynamic_slice x7, local copies, waits for them, and re-layouts, take(): return lax.dynamic_slice_in_dim(values, index * size, size, axis)  9.03 us
  transfers between devices with their start and end apart: 14, of which 7 were waited for; matrix products, arithmetic and copies ran while one was open for 15% of the time, Pallas kernels for 1%

commit v1 on v0

--- a/solution.py
+++ b/solution.py
@@ -153,7 +153,7 @@
     return whole
 
 
-def local(
+def plain(
     n_rep,
     n_fs,
     n_tp,
@@ -240,6 +240,674 @@
     return collect_rows(result, n_tp, tp)
 
 
+MESH = pl.DeviceIdType.MESH
+unit_tile = 256
+
+
+class Copies:
+    def __init__(self, send_sem):
+        self.send_sem = send_sem
+        self.made = []
+
+    def send(self, src, dst, recv_sem, device, cond=None, now=None):
+        index = len(self.made)
+        assert index < self.send_sem.shape[0]
+
+        def make():
+            return pltpu.make_async_remote_copy(
+                src_ref=src(),
+                dst_ref=dst(),
+                send_sem=self.send_sem.at[index],
+                recv_sem=recv_sem(),
+                device_id=device,
+                device_id_type=MESH,
+            )
+
+        self.made.append((make, cond))
+        guarded(both_of(cond, now), lambda: make().start())
+
+    def drain(self):
+        for make, cond in self.made:
+            guarded(cond, lambda make=make: make().wait_send())
+
+
+def guarded(cond, act):
+    if cond is None:
+        act()
+    else:
+        pl.when(cond)(lambda: act())
+
+
+def both_of(first, second):
+    if first is None or second is None:
+        return second if first is None else first
+    return jnp.logical_and(first, second)
+
+
+def rows_at(start, size):
+    if isinstance(start, int):
+        return pl.ds(start, size)
+    return pl.ds(pl.multiple_of(start, size), size)
+
+
+def send_count(n_z, chunks):
+    mixer = 4 + 10 * (n_z - 1)
+    weights = (chunks + 1) * (1 + 2 * (n_z - 1) + 2)
+    return mixer + weights + 1 + 4 + 3
+
+
+def layer_kernel(
+    n_z,
+    tokens,
+    mixer_gain,
+    mix_w,
+    taps,
+    offset,
+    recur_w,
+    recur_b,
+    input_w,
+    input_b,
+    rate,
+    out_w,
+    channel_gain,
+    gate_w,
+    up_w,
+    gate_taps,
+    gate_base,
+    down_w,
+    out,
+    tok,
+    mixb,
+    outb,
+    branch,
+    recurrent,
+    term_send,
+    term_recv,
+    term_own,
+    residual,
+    acts,
+    gub,
+    gub_swap,
+    dnb,
+    dnb_swap,
+    hid,
+    half_send,
+    half_recv,
+    half_own,
+    chip_own,
+    chip_send,
+    chip_recv,
+    result,
+    local_sem,
+    send_sem,
+    mix_sem,
+    gu_sem,
+    dn_sem,
+    term_sem,
+    act_sem,
+    half_send_sem,
+    half_recv_sem,
+    chip_send_sem,
+    chip_recv_sem,
+    out_send_sem,
+    out_recv_sem,
+):
+    x = lax.axis_index("rep")
+    f = lax.axis_index("fs")
+    t = lax.axis_index("tp")
+    z, y = f // 2, f % 2
+    n_f = 2 * n_z
+    length, width = tokens.shape
+    depth, channels = mix_w.shape
+    chunks = gub.shape[0]
+    units = chunks * unit_tile
+    half = length // 2
+    dim = recur_w.shape[1]
+
+    def at(x_at, z_at, y_at, t_at):
+        return (x_at, z_at * 2 + y_at, t_at)
+
+    other_x, other_y, other_t = 1 - x, 1 - y, 1 - t
+    near = {1: at(other_x, z, y, t), 2: at(x, z, other_y, t), 3: at(other_x, z, other_y, t)}
+    partner = at(x, z, y, other_t)
+    beside = z * 2 + other_y
+    column = [(z + step) % n_z for step in range(n_z)]
+    edge = n_z - 1
+    relay = n_z == 4
+    is_mid = jnp.logical_and(z > 0, z < edge) if relay else None
+    mid_from = edge - z
+    mid_blocks = [mid_from * 2 + y, mid_from * 2 + other_y]
+    mid_device = at(x, jnp.where(z == 1, 0, edge), y, t)
+
+    def direct(step):
+        if relay and step == 2:
+            return jnp.logical_not(is_mid)
+        return None
+
+    quarter = x * 2 + y
+    quarter_swap = x * 2 + other_y
+    local = []
+
+    def bring(src, dst):
+        copy = pltpu.make_async_copy(src, dst, local_sem.at[len(local)])
+        copy.start()
+        local.append(copy)
+        return copy
+
+    own_rows = rows_at(f * depth, depth)
+    got_mix = [bring(mix_w, mixb.at[own_rows, :]), bring(out_w, outb.at[:, own_rows])]
+
+    def unit_cols(which, chunk):
+        return rows_at(which * units + chunk * unit_tile, unit_tile)
+
+    low, high = pl.ds(0, unit_tile), pl.ds(unit_tile, unit_tile)
+    got_own, got_swap = [], []
+    for c in range(chunks):
+        got_own.append(
+            [
+                bring(gate_w.at[:, unit_cols(quarter, c)], gub.at[c, own_rows, low]),
+                bring(up_w.at[:, unit_cols(quarter, c)], gub.at[c, own_rows, high]),
+            ]
+        )
+        got_swap.append(
+            [
+                bring(gate_w.at[:, unit_cols(quarter_swap, c)], gub_swap.at[c, :, low]),
+                bring(up_w.at[:, unit_cols(quarter_swap, c)], gub_swap.at[c, :, high]),
+            ]
+        )
+    got_tok = [bring(tokens, tok)]
+    got_own.append([bring(down_w.at[rows_at(quarter * units, units), :], dnb.at[f])])
+    got_swap.append([bring(down_w.at[rows_at(quarter_swap * units, units), :], dnb_swap)])
+
+    barrier = pltpu.get_barrier_semaphore()
+    peers = [near[1], near[2], near[3], partner] + [at(x, w, y, t) for w in column[1:]]
+    for peer in peers:
+        pl.semaphore_signal(barrier, inc=1, device_id=peer, device_id_type=MESH)
+    pl.semaphore_wait(barrier, len(peers))
+
+    copies = Copies(send_sem)
+
+    def arrived(dst, sem, cond=None):
+        def wait():
+            copy = pltpu.make_async_remote_copy(
+                src_ref=dst(),
+                dst_ref=dst(),
+                send_sem=sem(),
+                recv_sem=sem(),
+                device_id=partner,
+                device_id_type=MESH,
+            )
+            copy.wait_recv()
+
+        guarded(cond, wait)
+
+    part_rows, part_out = depth // 2, channels // 2
+
+    def mix_pieces(block, part):
+        return [
+            (
+                lambda: mixb.at[rows_at(block * depth + part * part_rows, part_rows), :],
+                lambda: mix_sem.at[block, 2 * part],
+            ),
+            (
+                lambda: outb.at[rows_at(part * part_out, part_out), rows_at(block * depth, depth)],
+                lambda: mix_sem.at[block, 2 * part + 1],
+            ),
+        ]
+
+    def send_mix(block, part, device, cond=None):
+        for ref, sem in mix_pieces(block, part):
+            copies.send(ref, ref, sem, device, cond)
+
+    def wait_mix(block, part):
+        for ref, sem in mix_pieces(block, part):
+            arrived(ref, sem)
+
+    def weight_ref(stage, block):
+        if stage == chunks:
+            return lambda: dnb.at[block], lambda: dn_sem.at[block]
+        return lambda: gub.at[stage, rows_at(block * depth, depth), :], lambda: gu_sem.at[stage, block]
+
+    def send_swap(stage):
+        for copy in got_swap[stage]:
+            copy.wait()
+        ref, sem = weight_ref(stage, f)
+        copies.send(lambda: dnb_swap if stage == chunks else gub_swap.at[stage], ref, sem, near[2])
+
+    def send_own(stage):
+        for copy in got_own[stage]:
+            copy.wait()
+        ref, sem = weight_ref(stage, f)
+        for step in range(1, n_z):
+            copies.send(ref, ref, sem, at(x, column[step], y, t), direct(step))
+
+    def send_beside(stage):
+        ref, sem = weight_ref(stage, beside)
+        arrived(ref, sem)
+        for step in range(1, n_z):
+            copies.send(ref, ref, sem, at(x, column[step], y, t), direct(step))
+
+    def relay_block(stage, side, now=None):
+        if relay:
+            ref, sem = weight_ref(stage, mid_blocks[side])
+            arrived(ref, sem, both_of(is_mid, now))
+            copies.send(ref, ref, sem, mid_device, is_mid, now)
+
+    def wait_stage(stage, now=None):
+        for step in range(1, n_z):
+            for side in (y, other_y):
+                ref, sem = weight_ref(stage, column[step] * 2 + side)
+                fresh = None
+                if relay:
+                    fresh = jnp.logical_not(jnp.logical_and(is_mid, column[step] == mid_from))
+                arrived(ref, sem, both_of(fresh, now))
+
+    for copy in got_mix:
+        copy.wait()
+    for step in range(1, n_z):
+        send_mix(f, x, at(x, column[step], y, t), direct(step))
+    for part in range(2):
+        send_mix(f, part, near[2])
+    send_own(0)
+    send_swap(0)
+
+    def norm_rows(source, gain, dest, total, size=64):
+        def body(i, carry):
+            at_rows = rows_at(i * size, size)
+            widened = source[at_rows, :].astype(jnp.float32)
+            scaled = widened * lax.rsqrt(jnp.mean(widened * widened, axis=-1, keepdims=True) + epsilon)
+            dest[at_rows, :] = (scaled * gain[...]).astype(jnp.bfloat16)
+            return carry
+
+        lax.fori_loop(0, total // size, body, 0)
+
+    for copy in got_tok:
+        copy.wait()
+    norm_rows(tok, mixer_gain, acts.at[0], length)
+
+    order = [step for pair in zip(range(1, n_z), range(n_z - 1, 0, -1)) for step in pair][: n_z - 1]
+    for step in order:
+        block = column[step] * 2 + y
+        wait_mix(block, x)
+        send_mix(block, x, near[2])
+        send_mix(block, x, near[1])
+        if relay:
+            send_mix(block, x, mid_device, jnp.logical_and(is_mid, column[step] == mid_from))
+    for stage in range(1, chunks + 1):
+        send_swap(stage)
+    send_beside(0)
+    send_own(1)
+    for step in order:
+        block = column[step] * 2 + other_y
+        wait_mix(block, x)
+        send_mix(block, x, near[1])
+    send_beside(1)
+    relay_block(0, 0)
+    for stage in range(2, chunks):
+        send_own(stage)
+        send_beside(stage)
+    send_own(chunks)
+    relay_block(0, 1)
+    for part in range(2):
+        wait_mix(beside, part)
+    for step in order:
+        for side in (y, other_y):
+            wait_mix(column[step] * 2 + side, other_x)
+
+    def branch_body(j, carry):
+        cols = rows_at(j * 256, 256)
+        branch[:, cols] = (
+            jnp.dot(acts[0], mixb[:, cols], preferred_element_type=jnp.float32).astype(jnp.bfloat16).astype(jnp.float32)
+        )
+        return carry
+
+    lax.fori_loop(0, channels // 256, branch_body, 0)
+
+    def block_body(k, carry):
+        cols = rows_at(k * dim, dim)
+        recurrent[:, cols] = recur_block(
+            branch[:, cols],
+            taps[:, cols],
+            offset[:, cols],
+            recur_w[k],
+            recur_b[:, cols],
+            input_w[k],
+            input_b[:, cols],
+            rate[:, cols],
+        )
+        return carry
+
+    lax.fori_loop(0, channels // dim, block_body, 0)
+
+    def project(which, dest):
+        rows = rows_at(which * half, half)
+
+        def body(j, carry):
+            cols = rows_at(j * 512, 512)
+            dest[:, cols] = jnp.dot(recurrent[rows, :], outb[:, cols], preferred_element_type=jnp.float32).astype(
+                jnp.bfloat16
+            )
+            return carry
+
+        lax.fori_loop(0, width // 512, body, 0)
+
+    project(other_t, term_send)
+    copies.send(lambda: term_send, lambda: term_recv, lambda: term_sem.at[0], partner)
+    send_beside(chunks)
+    if chunks > 1:
+        relay_block(1, 0)
+    project(t, term_own)
+    arrived(lambda: term_recv, lambda: term_sem.at[0])
+    mine = rows_at(t * half, half)
+    theirs = rows_at(other_t * half, half)
+
+    def residual_body(i, carry):
+        rows = rows_at(i * 64, 64)
+        total = term_own[rows, :].astype(jnp.float32) + term_recv[rows, :].astype(jnp.float32)
+        base = tok[rows_at(t * half + i * 64, 64), :].astype(jnp.float32)
+        residual[rows, :] = (base + total).astype(jnp.bfloat16)
+        return carry
+
+    lax.fori_loop(0, half // 64, residual_body, 0)
+    norm_rows(residual, channel_gain, acts.at[0, mine, :], half)
+    def act_part(slot, rows):
+        return lambda: acts.at[slot, rows, :]
+
+    def act_arrival(slot, hop):
+        return lambda: act_sem.at[slot, hop]
+
+    for slot in (1, 2, 3):
+        copies.send(act_part(0, mine), act_part(slot, mine), act_arrival(slot, 0), near[slot])
+    copies.send(act_part(0, mine), act_part(0, mine), act_arrival(0, 1), partner)
+    if chunks > 1:
+        relay_block(1, 1)
+
+    def pass_on(slot, now):
+        arrived(act_part(slot, mine), act_arrival(slot, 0), now)
+        copies.send(act_part(slot, mine), act_part(slot, mine), act_arrival(slot, 1), partner, None, now)
+
+    def wait_acts(slot, now):
+        arrived(act_part(slot, theirs), act_arrival(slot, 1), now)
+
+    early = max(chunks - 1, 1)
+    plan = [(slot, c) for slot in range(4) for c in range(early)]
+    plan += [(slot, c) for c in range(early, chunks) for slot in range(4)]
+    hooks = [[] for _ in plan]
+    for number, (slot, c) in enumerate(plan):
+        if slot == 0:
+            hooks[number].append(functools.partial(wait_stage, c))
+        if c == 0:
+            hooks[number].append(functools.partial(wait_acts, slot))
+    for slot in (1, 2, 3):
+        hooks[slot * early - 1].append(functools.partial(pass_on, slot))
+    for stage in range(2, chunks + 1):
+        for side in range(2):
+            hooks[min(2 * stage - 2, len(plan) - 1)].append(functools.partial(relay_block, stage, side))
+
+    rows_iota = lax.broadcasted_iota(jnp.int32, (length, unit_tile), 0)
+
+    def gate_body(number, carry):
+        late = number >= 4 * early
+        slot = jnp.where(late, (number - 4 * early) % 4, number // early)
+        c = jnp.where(late, early + (number - 4 * early) // 4, number % early)
+        for index, acting in enumerate(hooks):
+            for act in acting:
+                act(now=number == index)
+
+        both = jnp.dot(acts[slot], gub[c], preferred_element_type=jnp.float32)
+        gate = both[:, :unit_tile].astype(jnp.bfloat16).astype(jnp.float32)
+        up = both[:, unit_tile:].astype(jnp.bfloat16).astype(jnp.float32)
+        cols = rows_at(quarter * units + c * unit_tile, unit_tile)
+        width_taps = gate_taps.shape[0]
+        mixed = gate_base[:, cols] + gate * gate_taps[width_taps - 1 : width_taps, cols]
+        for back in range(1, width_taps):
+            moved = jnp.where(rows_iota >= back, pltpu.roll(gate, back, 0), 0.0)
+            mixed = mixed + moved * gate_taps[width_taps - 1 - back : width_taps - back, cols]
+        hidden = (jax.nn.gelu(mixed) * up).astype(jnp.bfloat16)
+        place = rows_at(c * unit_tile, unit_tile)
+        rows = rows_at(slot * half, half)
+        hid[0, rows, place] = hidden[:half]
+        hid[1, rows, place] = hidden[half:]
+        return carry
+
+    lax.fori_loop(0, len(plan), gate_body, 0)
+
+    def block_of(i):
+        k = i // 2
+        if n_z == 4:
+            return (((z // 2 + k // 2) % 2) * 2 + (z % 2 + k % 2) % 2) * 2 + i % 2
+        return ((z + k) % n_z) * 2 + i % 2
+
+    def half_copy(i):
+        return pltpu.make_async_remote_copy(
+            src_ref=half_send.at[i],
+            dst_ref=half_recv.at[i],
+            send_sem=half_send_sem.at[i],
+            recv_sem=half_recv_sem.at[i],
+            device_id=partner,
+            device_id_type=MESH,
+        )
+
+    def chip_copy(i, slot):
+        return pltpu.make_async_remote_copy(
+            src_ref=chip_send.at[i, slot - 1],
+            dst_ref=chip_recv.at[i, slot - 1],
+            send_sem=chip_send_sem.at[i, slot - 1],
+            recv_sem=chip_recv_sem.at[i, slot - 1],
+            device_id=near[slot],
+            device_id_type=MESH,
+        )
+
+    def out_copy(i):
+        part = result.at[mine, rows_at(block_of(i) * depth, depth)]
+        return pltpu.make_async_remote_copy(
+            src_ref=part,
+            dst_ref=part,
+            send_sem=out_send_sem.at[i],
+            recv_sem=out_recv_sem.at[i],
+            device_id=partner,
+            device_id_type=MESH,
+        )
+
+    lag = 3
+
+    def down_body(i, carry):
+        @pl.when(i < n_f)
+        def _():
+            block = block_of(i)
+            known = jnp.logical_or(block == f, block == beside)
+            if relay:
+                known = jnp.logical_or(known, jnp.logical_and(is_mid, block // 2 == mid_from))
+            arrived(lambda: dnb.at[block], lambda: dn_sem.at[block], jnp.logical_not(known))
+            half_send[i] = jnp.dot(hid[other_t], dnb[block], preferred_element_type=jnp.float32).astype(jnp.bfloat16)
+            half_copy(i).start()
+            half_own[i % 2] = jnp.dot(hid[t], dnb[block], preferred_element_type=jnp.float32).astype(jnp.bfloat16)
+
+        j = i - 1
+
+        @pl.when(jnp.logical_and(j >= 0, j < n_f))
+        def _():
+            half_copy(j).wait_recv()
+
+            def add(slot):
+                rows = pl.ds(slot * half, half)
+                return half_own[j % 2, rows, :].astype(jnp.float32) + half_recv[j, rows, :].astype(jnp.float32)
+
+            for slot in (3, 1, 2):
+                chip_send[j, slot - 1] = add(slot).astype(jnp.bfloat16)
+            for slot in (1, 2, 3):
+                chip_copy(j, slot).start()
+            chip_own[j] = add(0)
+
+        m = i - lag
+
+        @pl.when(m >= 0)
+        def _():
+            for slot in (1, 2, 3):
+                chip_copy(m, slot).wait_recv()
+            cols = rows_at(block_of(m) * depth, depth)
+            total = chip_own[m]
+            for slot in range(3):
+                total = total + chip_recv[m, slot].astype(jnp.float32)
+            result[mine, cols] = (residual[:, cols].astype(jnp.float32) + total).astype(jnp.bfloat16)
+            out_copy(m).start()
+
+        return carry
+
+    lax.fori_loop(0, n_f + lag, down_body, 0)
+
+    def drain_body(i, carry):
+        out_copy(i).wait_send()
+        half_copy(i).wait_send()
+        for slot in (1, 2, 3):
+            chip_copy(i, slot).wait_send()
+        arrived(
+            lambda: result.at[theirs, rows_at(block_of(i) * depth, depth)],
+            lambda: out_recv_sem.at[i],
+        )
+        return carry
+
+    lax.fori_loop(0, n_f, drain_body, 0)
+    copies.drain()
+    last = pltpu.make_async_copy(result, out, local_sem.at[len(local)])
+    last.start()
+    last.wait()
+
+
+def recur_block(branch, taps, offset, recur_weight, recur_bias, input_weight, input_bias, rate):
+    length = branch.shape[0]
+    width = taps.shape[0]
+    rows = lax.broadcasted_iota(jnp.int32, branch.shape, 0)
+
+    def shifted(values, step, fill):
+        return jnp.where(rows >= step, pltpu.roll(values, step, 0), fill)
+
+    total = offset + branch * taps[width - 1 : width, :]
+    for back in range(1, width):
+        total = total + shifted(branch, back, 0.0) * taps[width - 1 - back : width - back, :]
+    smoothed = total.astype(jnp.bfloat16)
+    recur = jnp.dot(smoothed, recur_weight, preferred_element_type=jnp.float32)
+    recur_gate = jax.nn.sigmoid(recur + recur_bias)
+    gated = jnp.dot(smoothed, input_weight, preferred_element_type=jnp.float32)
+    input_gate = jax.nn.sigmoid(gated + input_bias)
+    log_decay = recur_gate * rate
+    state = jnp.sqrt(one_minus_exp(2.0 * log_decay)) * (input_gate * smoothed.astype(jnp.float32))
+    decay = jnp.exp(log_decay)
+    step = 1
+    while step < length:
+        state = state + decay * shifted(state, step, 0.0)
+        if 2 * step < length:
+            decay = decay * shifted(decay, step, 1.0)
+        step *= 2
+    return state.astype(jnp.bfloat16)
+
+
+def fused(
+    n_fs,
+    tokens,
+    mixer_gain,
+    mix_weight,
+    mixer_conv,
+    mixer_offset,
+    recur_weight,
+    recur_bias,
+    input_weight,
+    input_bias,
+    decay_logit,
+    out_weight,
+    channel_gain,
+    gate_weight,
+    up_weight,
+    gate_conv,
+    gate_offset,
+    down_weight,
+):
+    n_z = n_fs // 2
+    length, width = tokens.shape
+    depth, channels = mix_weight.shape
+    units = gate_weight.shape[1] // 4
+    chunks = units // unit_tile
+    half = length // 2
+    row = lambda v: v.reshape(1, v.shape[0])
+    hbm = pl.BlockSpec(memory_space=pl.ANY)
+    vmem = pl.BlockSpec(memory_space=pltpu.VMEM)
+    bf16, f32 = jnp.bfloat16, jnp.float32
+    dma = pltpu.SemaphoreType.DMA
+    return pl.pallas_call(
+        functools.partial(layer_kernel, n_z),
+        name="layer",
+        in_specs=[hbm, vmem, hbm] + [vmem] * 7 + [hbm, vmem, hbm, hbm, vmem, vmem, hbm],
+        out_specs=hbm,
+        out_shape=jax.ShapeDtypeStruct((length, width), bf16),
+        scratch_shapes=[
+            pltpu.VMEM((length, width), bf16),
+            pltpu.VMEM((width, channels), bf16),
+            pltpu.VMEM((channels, width), bf16),
+            pltpu.VMEM((length, channels), f32),
+            pltpu.VMEM((length, channels), bf16),
+            pltpu.VMEM((half, width), bf16),
+            pltpu.VMEM((half, width), bf16),
+            pltpu.VMEM((half, width), bf16),
+            pltpu.VMEM((half, width), bf16),
+            pltpu.VMEM((4, length, width), bf16),
+            pltpu.VMEM((chunks, width, 2 * unit_tile), bf16),
+            pltpu.VMEM((chunks, depth, 2 * unit_tile), bf16),
+            pltpu.VMEM((n_fs, units, depth), bf16),
+            pltpu.VMEM((units, depth), bf16),
+            pltpu.VMEM((2, 4 * half, units), bf16),
+            pltpu.VMEM((n_fs, 4 * half, depth), bf16),
+            pltpu.VMEM((n_fs, 4 * half, depth), bf16),
+            pltpu.VMEM((2, 4 * half, depth), bf16),
+            pltpu.VMEM((n_fs, half, depth), f32),
+            pltpu.VMEM((n_fs, 3, half, depth), bf16),
+            pltpu.VMEM((n_fs, 3, half, depth), bf16),
+            pltpu.VMEM((length, width), bf16),
+            dma((6 + 4 * chunks,)),
+            dma((send_count(n_z, chunks),)),
+            dma((n_fs, 4)),
+            dma((chunks, n_fs)),
+            dma((n_fs,)),
+            dma((1,)),
+            dma((4, 2)),
+            dma((n_fs,)),
+            dma((n_fs,)),
+            dma((n_fs, 3)),
+            dma((n_fs, 3)),
+            dma((n_fs,)),
+            dma((n_fs,)),
+        ],
+        compiler_params=pltpu.CompilerParams(
+            collective_id=0, has_side_effects=True, vmem_limit_bytes=60 * 2**20
+        ),
+    )(
+        tokens,
+        row(mixer_gain),
+        mix_weight,
+        mixer_conv,
+        row(mixer_offset),
+        recur_weight,
+        row(recur_bias),
+        input_weight,
+        row(input_bias),
+        row(lru_scale * jax.nn.log_sigmoid(decay_logit)),
+        out_weight,
+        row(channel_gain),
+        gate_weight,
+        up_weight,
+        gate_conv,
+        row(gate_offset),
+        down_weight,
+    )
+
+
+def local(n_rep, n_fs, n_tp, *arrays):
+    units, columns = arrays[16].shape
+    fits = n_rep == 2 and n_tp == 2 and n_fs % 2 == 0 and n_fs <= 8
+    if fits and units % (4 * unit_tile) == 0 and columns % 128 == 0:
+        return fused(n_fs, *arrays)
+    return plain(n_rep, n_fs, n_tp, *arrays)
+
+
 def solution(mesh):
     in_specs = (
         P(("rep", "fs"), None),

time: 423 us -> 249 us (0.59)
  the two profiles are of different devices: /device:TPU:0 before, /device:TPU:9 now
where the time goes in v1:
time: 249 us
  Pallas kernels  245 us (98%)
  local copies, waits for them, and re-layouts  3.16 us (1%)
    pallas_call x1, Pallas kernels, fused(): pl.pallas_call(functools.partial(layer_kernel, n_z), name='layer', in_spe...  245 us

profile of v1, /device:TPU:9, one launch (start us, length us, event | category | flops | bytes accessed | tf_op | source)
XLA Modules:
  0.0 249.2 jit_solution(13557151893909020945)
XLA Ops:
  0.0 1.3 fusion.1
  1.3 244.7 %layer.1 = bf16[512,2048]{1,0:T(8,128)(2,1)} custom-call(bf16[512,2048]{1,0:T(8,128)(2,1)} %tokens.1, f32[1,2048]{1,0:T(1,128)} %bitcast.8, bf16[256,512]{1,0:T(8,128)(2,1)} %mix_w.1, f32[4,512]{1,0:T(4,128)} %taps.1, f32[1,512]{1,0:T(1,128)} %bitcast.11, bf16[4,128,128]{2,1,0:T(8,128)(2,1)} %recur_w.1, f32[1,512]{1,0:T(1,128)} %bitcast.12, ...), custom_call_target="tpu_custom_call" | custom-call | tf_op jit(solution)/shard_map/layer/pallas_call | solution.py:836
  246.0 3.2 %copy.19 = bf16[512,2048]{1,0:T(8,128)(2,1)} copy(bf16[512,2048]{1,0:T(8,128)(2,1)} %layer.1) | data formatting | bytes 4194304

commit v2 on v1

--- a/solution.py
+++ b/solution.py
@@ -242,6 +242,7 @@
 
 MESH = pl.DeviceIdType.MESH
 unit_tile = 256
+pieces = 2
 
 
 class Copies:
@@ -292,8 +293,8 @@
 
 def send_count(n_z, chunks):
     mixer = 4 + 10 * (n_z - 1)
-    weights = (chunks + 1) * (1 + 2 * (n_z - 1) + 2)
-    return mixer + weights + 1 + 4 + 3
+    weights = chunks + 1 + (chunks + pieces) * (2 * (n_z - 1) + 4)
+    return mixer + weights + 9
 
 
 def layer_kernel(
@@ -307,7 +308,7 @@
     recur_b,
     input_w,
     input_b,
-    rate,
+    logit,
     out_w,
     channel_gain,
     gate_w,
@@ -351,6 +352,7 @@
     chip_recv_sem,
     out_send_sem,
     out_recv_sem,
+    write_sem,
 ):
     x = lax.axis_index("rep")
     f = lax.axis_index("fs")
@@ -371,18 +373,22 @@
     near = {1: at(other_x, z, y, t), 2: at(x, z, other_y, t), 3: at(other_x, z, other_y, t)}
     partner = at(x, z, y, other_t)
     beside = z * 2 + other_y
-    column = [(z + step) % n_z for step in range(n_z)]
+    relay = n_z == 4
+    toward = jnp.where(2 * z < n_z, 1, n_z - 1)
+    column = [(z + step * (toward if relay else 1)) % n_z for step in range(n_z)]
     edge = n_z - 1
-    relay = n_z == 4
     is_mid = jnp.logical_and(z > 0, z < edge) if relay else None
-    mid_from = edge - z
-    mid_blocks = [mid_from * 2 + y, mid_from * 2 + other_y]
-    mid_device = at(x, jnp.where(z == 1, 0, edge), y, t)
+    mid_from = column[1:3]
+    mid_to = column[edge]
+    mid_device = at(x, mid_to, y, t)
+
+    def relayed(z_at):
+        return jnp.logical_and(is_mid, z_at != mid_to)
 
     def direct(step):
-        if relay and step == 2:
-            return jnp.logical_not(is_mid)
-        return None
+        if not relay or step == 1:
+            return None
+        return jnp.logical_not(is_mid) if step == 2 else is_mid
 
     quarter = x * 2 + y
     quarter_swap = x * 2 + other_y
@@ -465,7 +471,7 @@
 
     def weight_ref(stage, block):
         if stage == chunks:
-            return lambda: dnb.at[block], lambda: dn_sem.at[block]
+            return lambda: dnb.at[block], lambda: dn_sem.at[block, 0]
         return lambda: gub.at[stage, rows_at(block * depth, depth), :], lambda: gu_sem.at[stage, block]
 
     def send_swap(stage):
@@ -474,24 +480,61 @@
         ref, sem = weight_ref(stage, f)
         copies.send(lambda: dnb_swap if stage == chunks else gub_swap.at[stage], ref, sem, near[2])
 
+    def send_block(stage, block, steps=range(1, n_z), also=None):
+        ref, sem = weight_ref(stage, block)
+        for step in steps:
+            copies.send(ref, ref, sem, at(x, column[step], y, t), both_of(direct(step), also))
+
     def send_own(stage):
         for copy in got_own[stage]:
             copy.wait()
-        ref, sem = weight_ref(stage, f)
-        for step in range(1, n_z):
-            copies.send(ref, ref, sem, at(x, column[step], y, t), direct(step))
+        send_block(stage, f)
+
+    def send_first(inner):
+        if not inner:
+            for copy in got_own[0]:
+                copy.wait()
+            send_block(0, f, range(2 if relay else 1, n_z))
+        if relay:
+            send_block(0, f, range(1, 2), is_mid if inner else jnp.logical_not(is_mid))
 
     def send_beside(stage):
-        ref, sem = weight_ref(stage, beside)
-        arrived(ref, sem)
-        for step in range(1, n_z):
-            copies.send(ref, ref, sem, at(x, column[step], y, t), direct(step))
-
-    def relay_block(stage, side, now=None):
+        arrived(*weight_ref(stage, beside))
+        send_block(stage, beside)
+
+    piece_width = depth // pieces
+
+    def down_ref(block, piece):
+        cols = rows_at(piece * piece_width, piece_width)
+        return lambda: dnb.at[block, :, cols], lambda: dn_sem.at[block, piece]
+
+    def send_down():
+        for copy in got_own[chunks]:
+            copy.wait()
+        arrived(*weight_ref(chunks, beside))
+        for side in range(2):
+            for piece in range(pieces):
+                ref, sem = down_ref(z * 2 + side, piece)
+                for step in range(1, n_z):
+                    copies.send(ref, ref, sem, at(x, column[step], y, t), direct(step))
+
+    side_blocks = [[z_at * 2 + side for z_at in mid_from] for side in (y, other_y)]
+    mid_blocks = [[z_at * 2 + side for side in range(2)] for z_at in mid_from]
+
+    def relay_ref(ref, sem, now):
+        arrived(ref, sem, both_of(is_mid, now))
+        copies.send(ref, ref, sem, mid_device, is_mid, now)
+
+    def relay_blocks(stage, blocks, now=None):
         if relay:
-            ref, sem = weight_ref(stage, mid_blocks[side])
-            arrived(ref, sem, both_of(is_mid, now))
-            copies.send(ref, ref, sem, mid_device, is_mid, now)
+            for block in blocks:
+                relay_ref(*weight_ref(stage, block), now)
+
+    def relay_down(blocks, now=None):
+        if relay:
+            for block in blocks:
+                for piece in range(pieces):
+                    relay_ref(*down_ref(block, piece), now)
 
     def wait_stage(stage, now=None):
         for step in range(1, n_z):
@@ -499,7 +542,7 @@
                 ref, sem = weight_ref(stage, column[step] * 2 + side)
                 fresh = None
                 if relay:
-                    fresh = jnp.logical_not(jnp.logical_and(is_mid, column[step] == mid_from))
+                    fresh = jnp.logical_not(is_mid) if step < edge else None
                 arrived(ref, sem, both_of(fresh, now))
 
     for copy in got_mix:
@@ -508,7 +551,7 @@
         send_mix(f, x, at(x, column[step], y, t), direct(step))
     for part in range(2):
         send_mix(f, part, near[2])
-    send_own(0)
+    send_first(False)
     send_swap(0)
 
     def norm_rows(source, gain, dest, total, size=64):
@@ -525,35 +568,31 @@
         copy.wait()
     norm_rows(tok, mixer_gain, acts.at[0], length)
 
-    order = [step for pair in zip(range(1, n_z), range(n_z - 1, 0, -1)) for step in pair][: n_z - 1]
+    order = range(1, n_z)
     for step in order:
         block = column[step] * 2 + y
         wait_mix(block, x)
         send_mix(block, x, near[2])
         send_mix(block, x, near[1])
-        if relay:
-            send_mix(block, x, mid_device, jnp.logical_and(is_mid, column[step] == mid_from))
+        if relay and step < edge:
+            send_mix(block, x, mid_device, is_mid)
+    send_first(True)
     for stage in range(1, chunks + 1):
         send_swap(stage)
     send_beside(0)
+    relay_blocks(0, side_blocks[0])
     send_own(1)
     for step in order:
         block = column[step] * 2 + other_y
         wait_mix(block, x)
         send_mix(block, x, near[1])
+    relay_blocks(0, side_blocks[1])
     send_beside(1)
-    relay_block(0, 0)
-    for stage in range(2, chunks):
-        send_own(stage)
-        send_beside(stage)
-    send_own(chunks)
-    relay_block(0, 1)
     for part in range(2):
         wait_mix(beside, part)
     for step in order:
         for side in (y, other_y):
             wait_mix(column[step] * 2 + side, other_x)
-
     def branch_body(j, carry):
         cols = rows_at(j * 256, 256)
         branch[:, cols] = (
@@ -573,11 +612,15 @@
             recur_b[:, cols],
             input_w[k],
             input_b[:, cols],
-            rate[:, cols],
+            lru_scale * log_sigmoid(logit[:, cols]),
         )
         return carry
 
     lax.fori_loop(0, channels // dim, block_body, 0)
+
+    relay_blocks(1, side_blocks[0])
+    send_own(2)
+    send_beside(2)
 
     def project(which, dest):
         rows = rows_at(which * half, half)
@@ -593,9 +636,6 @@
 
     project(other_t, term_send)
     copies.send(lambda: term_send, lambda: term_recv, lambda: term_sem.at[0], partner)
-    send_beside(chunks)
-    if chunks > 1:
-        relay_block(1, 0)
     project(t, term_own)
     arrived(lambda: term_recv, lambda: term_sem.at[0])
     mine = rows_at(t * half, half)
@@ -619,8 +659,10 @@
     for slot in (1, 2, 3):
         copies.send(act_part(0, mine), act_part(slot, mine), act_arrival(slot, 0), near[slot])
     copies.send(act_part(0, mine), act_part(0, mine), act_arrival(0, 1), partner)
-    if chunks > 1:
-        relay_block(1, 1)
+    relay_blocks(1, side_blocks[1])
+    relay_blocks(2, side_blocks[0])
+    relay_blocks(2, side_blocks[1])
+    send_down()
 
     def pass_on(slot, now):
         arrived(act_part(slot, mine), act_arrival(slot, 0), now)
@@ -640,9 +682,6 @@
             hooks[number].append(functools.partial(wait_acts, slot))
     for slot in (1, 2, 3):
         hooks[slot * early - 1].append(functools.partial(pass_on, slot))
-    for stage in range(2, chunks + 1):
-        for side in range(2):
-            hooks[min(2 * stage - 2, len(plan) - 1)].append(functools.partial(relay_block, stage, side))
 
     rows_iota = lax.broadcasted_iota(jnp.int32, (length, unit_tile), 0)
 
@@ -671,18 +710,24 @@
         return carry
 
     lax.fori_loop(0, len(plan), gate_body, 0)
+    relay_down(mid_blocks[0])
+
+    n_b = n_f * pieces
 
     def block_of(i):
-        k = i // 2
+        k, side = i // (2 * pieces), (i // pieces) % 2
         if n_z == 4:
-            return (((z // 2 + k // 2) % 2) * 2 + (z % 2 + k % 2) % 2) * 2 + i % 2
-        return ((z + k) % n_z) * 2 + i % 2
+            return (((z // 2 + k // 2) % 2) * 2 + (z % 2 + k % 2) % 2) * 2 + side
+        return ((z + k) % n_z) * 2 + side
+
+    def cols_of(i):
+        return rows_at((block_of(i) * pieces + i % pieces) * piece_width, piece_width)
 
     def half_copy(i):
         return pltpu.make_async_remote_copy(
             src_ref=half_send.at[i],
             dst_ref=half_recv.at[i],
-            send_sem=half_send_sem.at[i],
+            send_sem=half_send_sem.at[0],
             recv_sem=half_recv_sem.at[i],
             device_id=partner,
             device_id_type=MESH,
@@ -692,86 +737,94 @@
         return pltpu.make_async_remote_copy(
             src_ref=chip_send.at[i, slot - 1],
             dst_ref=chip_recv.at[i, slot - 1],
-            send_sem=chip_send_sem.at[i, slot - 1],
-            recv_sem=chip_recv_sem.at[i, slot - 1],
+            send_sem=chip_send_sem.at[0],
+            recv_sem=chip_recv_sem.at[i],
             device_id=near[slot],
             device_id_type=MESH,
         )
 
     def out_copy(i):
-        part = result.at[mine, rows_at(block_of(i) * depth, depth)]
         return pltpu.make_async_remote_copy(
-            src_ref=part,
-            dst_ref=part,
-            send_sem=out_send_sem.at[i],
-            recv_sem=out_recv_sem.at[i],
+            src_ref=result.at[:, cols_of(i)],
+            dst_ref=out.at[mine, cols_of(i)],
+            send_sem=out_send_sem.at[0],
+            recv_sem=out_recv_sem.at[0],
             device_id=partner,
             device_id_type=MESH,
         )
 
+    def write_copy(i):
+        return pltpu.make_async_copy(result.at[:, cols_of(i)], out.at[mine, cols_of(i)], write_sem.at[0])
+
     lag = 3
 
     def down_body(i, carry):
-        @pl.when(i < n_f)
-        def _():
-            block = block_of(i)
-            known = jnp.logical_or(block == f, block == beside)
-            if relay:
-                known = jnp.logical_or(known, jnp.logical_and(is_mid, block // 2 == mid_from))
-            arrived(lambda: dnb.at[block], lambda: dn_sem.at[block], jnp.logical_not(known))
-            half_send[i] = jnp.dot(hid[other_t], dnb[block], preferred_element_type=jnp.float32).astype(jnp.bfloat16)
-            half_copy(i).start()
-            half_own[i % 2] = jnp.dot(hid[t], dnb[block], preferred_element_type=jnp.float32).astype(jnp.bfloat16)
-
-        j = i - 1
-
-        @pl.when(jnp.logical_and(j >= 0, j < n_f))
-        def _():
-            half_copy(j).wait_recv()
-
-            def add(slot):
-                rows = pl.ds(slot * half, half)
-                return half_own[j % 2, rows, :].astype(jnp.float32) + half_recv[j, rows, :].astype(jnp.float32)
-
-            for slot in (3, 1, 2):
-                chip_send[j, slot - 1] = add(slot).astype(jnp.bfloat16)
-            for slot in (1, 2, 3):
-                chip_copy(j, slot).start()
-            chip_own[j] = add(0)
-
-        m = i - lag
-
-        @pl.when(m >= 0)
-        def _():
-            for slot in (1, 2, 3):
-                chip_copy(m, slot).wait_recv()
-            cols = rows_at(block_of(m) * depth, depth)
-            total = chip_own[m]
-            for slot in range(3):
-                total = total + chip_recv[m, slot].astype(jnp.float32)
-            result[mine, cols] = (residual[:, cols].astype(jnp.float32) + total).astype(jnp.bfloat16)
-            out_copy(m).start()
-
+        relay_down(mid_blocks[1], i == 2 * pieces)
+
+        block, cols = block_of(i), rows_at((i % pieces) * piece_width, piece_width)
+        fresh = jnp.logical_and(block != f, block != beside)
+        if relay:
+            fresh = jnp.logical_and(fresh, jnp.logical_not(relayed(block // 2)))
+        arrived(lambda: dnb.at[block, :, cols], lambda: dn_sem.at[block, i % pieces], fresh)
+        weight = dnb[block, :, cols]
+        half_send[i] = jnp.dot(hid[other_t], weight, preferred_element_type=jnp.float32).astype(jnp.bfloat16)
+        half_copy(i).start()
+        half_own[...] = jnp.dot(hid[t], weight, preferred_element_type=jnp.float32).astype(jnp.bfloat16)
+        half_copy(i).wait_recv()
+
+        def add(slot):
+            rows = pl.ds(slot * half, half)
+            return half_own[rows, :].astype(jnp.float32) + half_recv[i, rows, :].astype(jnp.float32)
+
+        before = None
+        for slot in (3, 1, 2):
+            chip_send[i, slot - 1] = add(slot).astype(jnp.bfloat16)
+            if before is not None:
+                chip_copy(i, before).start()
+            before = slot
+        chip_own[i] = add(0)
+        chip_copy(i, before).start()
+
+        pl.when(i >= lag)(lambda: finish(i - lag))
         return carry
 
-    lax.fori_loop(0, n_f + lag, down_body, 0)
-
-    def drain_body(i, carry):
-        out_copy(i).wait_send()
-        half_copy(i).wait_send()
-        for slot in (1, 2, 3):
-            chip_copy(i, slot).wait_send()
-        arrived(
-            lambda: result.at[theirs, rows_at(block_of(i) * depth, depth)],
-            lambda: out_recv_sem.at[i],
-        )
+    def finish(m):
+        arrived(lambda: chip_recv.at[m], lambda: chip_recv_sem.at[m])
+        total = chip_own[m]
+        for slot in range(3):
+            total = total + chip_recv[m, slot].astype(jnp.float32)
+        result[:, cols_of(m)] = (residual[:, cols_of(m)].astype(jnp.float32) + total).astype(jnp.bfloat16)
+        out_copy(m).start()
+        write_copy(m).start()
+
+    def finish_body(m, carry):
+        finish(m)
         return carry
 
-    lax.fori_loop(0, n_f, drain_body, 0)
+    lax.fori_loop(0, n_b, down_body, 0)
     copies.drain()
-    last = pltpu.make_async_copy(result, out, local_sem.at[len(local)])
-    last.start()
-    last.wait()
+    lax.fori_loop(n_b - lag, n_b, finish_body, 0)
+
+    def sent(ref, sem):
+        pltpu.make_async_remote_copy(
+            src_ref=ref, dst_ref=ref, send_sem=sem, recv_sem=sem, device_id=partner, device_id_type=MESH
+        ).wait_send()
+
+    sent(half_send, half_send_sem.at[0])
+    sent(chip_send, chip_send_sem.at[0])
+    sent(result, out_send_sem.at[0])
+    pltpu.make_async_copy(result, out.at[mine, :], write_sem.at[0]).wait()
+    arrived(lambda: out.at[theirs, :], lambda: out_recv_sem.at[0])
+
+
+def log_sigmoid(v):
+    small = jnp.exp(-jnp.abs(v))
+    ratio = small / (2.0 + small)
+    square = ratio * ratio
+    series = 1.0 / 15.0
+    for order in (13.0, 11.0, 9.0, 7.0, 5.0, 3.0, 1.0):
+        series = 1.0 / order + square * series
+    return jnp.minimum(v, 0.0) - 2.0 * ratio * series
 
 
 def recur_block(branch, taps, offset, recur_weight, recur_bias, input_weight, input_bias, rate):
@@ -828,12 +881,13 @@
     units = gate_weight.shape[1] // 4
     chunks = units // unit_tile
     half = length // 2
+    n_b = n_fs * pieces
     row = lambda v: v.reshape(1, v.shape[0])
     hbm = pl.BlockSpec(memory_space=pl.ANY)
     vmem = pl.BlockSpec(memory_space=pltpu.VMEM)
     bf16, f32 = jnp.bfloat16, jnp.float32
     dma = pltpu.SemaphoreType.DMA
-    return pl.pallas_call(
+    rows_out = pl.pallas_call(
         functools.partial(layer_kernel, n_z),
         name="layer",
         in_specs=[hbm, vmem, hbm] + [vmem] * 7 + [hbm, vmem, hbm, hbm, vmem, vmem, hbm],
@@ -855,29 +909,30 @@
             pltpu.VMEM((n_fs, units, depth), bf16),
             pltpu.VMEM((units, depth), bf16),
             pltpu.VMEM((2, 4 * half, units), bf16),
-            pltpu.VMEM((n_fs, 4 * half, depth), bf16),
-            pltpu.VMEM((n_fs, 4 * half, depth), bf16),
-            pltpu.VMEM((2, 4 * half, depth), bf16),
-            pltpu.VMEM((n_fs, half, depth), f32),
-            pltpu.VMEM((n_fs, 3, half, depth), bf16),
-            pltpu.VMEM((n_fs, 3, half, depth), bf16),
-            pltpu.VMEM((length, width), bf16),
-            dma((6 + 4 * chunks,)),
+            pltpu.VMEM((n_b, 4 * half, depth // pieces), bf16),
+            pltpu.VMEM((n_b, 4 * half, depth // pieces), bf16),
+            pltpu.VMEM((4 * half, depth // pieces), bf16),
+            pltpu.VMEM((n_b, half, depth // pieces), f32),
+            pltpu.VMEM((n_b, 3, half, depth // pieces), bf16),
+            pltpu.VMEM((n_b, 3, half, depth // pieces), bf16),
+            pltpu.VMEM((half, width), bf16),
+            dma((5 + 4 * chunks,)),
             dma((send_count(n_z, chunks),)),
             dma((n_fs, 4)),
             dma((chunks, n_fs)),
-            dma((n_fs,)),
+            dma((n_fs, pieces)),
             dma((1,)),
             dma((4, 2)),
-            dma((n_fs,)),
-            dma((n_fs,)),
-            dma((n_fs, 3)),
-            dma((n_fs, 3)),
-            dma((n_fs,)),
-            dma((n_fs,)),
+            dma((1,)),
+            dma((n_b,)),
+            dma((1,)),
+            dma((n_b,)),
+            dma((1,)),
+            dma((1,)),
+            dma((1,)),
         ],
         compiler_params=pltpu.CompilerParams(
-            collective_id=0, has_side_effects=True, vmem_limit_bytes=60 * 2**20
+            collective_id=0, has_side_effects=True, vmem_limit_bytes=56 * 2**20
         ),
     )(
         tokens,
@@ -889,7 +944,7 @@
         row(recur_bias),
         input_weight,
         row(input_bias),
-        row(lru_scale * jax.nn.log_sigmoid(decay_logit)),
+        row(decay_logit),
         out_weight,
         row(channel_gain),
         gate_weight,
@@ -898,12 +953,39 @@
         row(gate_offset),
         down_weight,
     )
+    parts = 4
+    return pl.pallas_call(
+        write_out,
+        name="write_out",
+        in_specs=[pl.BlockSpec(memory_space=pltpu.HBM)],
+        out_specs=pl.BlockSpec(memory_space=pltpu.HBM),
+        out_shape=jax.ShapeDtypeStruct((length, width), bf16),
+        scratch_shapes=[pltpu.VMEM((parts, length // parts, width), bf16), dma((2, parts))],
+        compiler_params=pltpu.CompilerParams(vmem_limit_bytes=62 * 2**20),
+    )(rows_out)
+
+
+def write_out(rows_ref, out_ref, held, sem):
+    parts, size, _ = held.shape
+    copies_in = [
+        pltpu.make_async_copy(rows_ref.at[pl.ds(k * size, size), :], held.at[k], sem.at[0, k]) for k in range(parts)
+    ]
+    copies_out = [
+        pltpu.make_async_copy(held.at[k], out_ref.at[pl.ds(k * size, size), :], sem.at[1, k]) for k in range(parts)
+    ]
+    for copy in copies_in:
+        copy.start()
+    for k in range(parts):
+        copies_in[k].wait()
+        copies_out[k].start()
+    for copy in copies_out:
+        copy.wait()
 
 
 def local(n_rep, n_fs, n_tp, *arrays):
     units, columns = arrays[16].shape
     fits = n_rep == 2 and n_tp == 2 and n_fs % 2 == 0 and n_fs <= 8
-    if fits and units % (4 * unit_tile) == 0 and columns % 128 == 0:
+    if fits and units == 12 * unit_tile and columns % 128 == 0:
         return fused(n_fs, *arrays)
     return plain(n_rep, n_fs, n_tp, *arrays)
 

time: 249 us -> 189 us (0.76)
  the two profiles are of different devices: /device:TPU:9 before, /device:TPU:0 now
where the time goes in v2:
time: 189 us
  Pallas kernels  189 us (100%)
    pallas_call x1, Pallas kernels, fused(): pl.pallas_call(functools.partial(layer_kernel, n_z), name='layer', in_spe...  187 us

profile of v2, /device:TPU:0, one launch (start us, length us, event | category | flops | bytes accessed | tf_op | source)
XLA Modules:
  0.0 189.0 jit_solution(13094472046861642685)
XLA Ops:
  0.0 186.5 %layer.1.rows_ref = bf16[512,2048]{1,0:T(8,128)(2,1)} custom-call(bf16[512,2048]{1,0:T(8,128)(2,1)} %tokens.1, f32[1,2048]{1,0:T(1,128)} %bitcast.8, bf16[256,512]{1,0:T(8,128)(2,1)} %mix_w.1, f32[4,512]{1,0:T(4,128)} %taps.1, f32[1,512]{1,0:T(1,128)} %bitcast.10, bf16[4,128,128]{2,1,0:T(8,128)(2,1)} %recur_w.1, f32[1,512]{1,0:T(1,128)} %bitcast.11, ...), custom_call_target="tpu_custom_call" | custom-call | tf_op jit(solution)/shard_map/layer/pallas_call | solution.py:890
  186.5 2.4 %write_out.1 = bf16[512,2048]{1,0:T(8,128)(2,1)} custom-call(bf16[512,2048]{1,0:T(8,128)(2,1)} %layer.1.rows_ref), custom_call_target="tpu_custom_call" | custom-call | tf_op jit(solution)/shard_map/write_out/pallas_call | solution.py:957

commit v3 on v2

--- a/solution.py
+++ b/solution.py
@@ -1,4 +1,6 @@
 import functools
+import itertools
+import math
 
 import jax
 import jax.numpy as jnp
@@ -246,30 +248,55 @@
 
 
 class Copies:
-    def __init__(self, send_sem):
+    def __init__(self, send_sem, is_mid):
         self.send_sem = send_sem
-        self.made = []
-
-    def send(self, src, dst, recv_sem, device, cond=None, now=None):
-        index = len(self.made)
-        assert index < self.send_sem.shape[0]
-
-        def make():
-            return pltpu.make_async_remote_copy(
+        self.conds = {"all": None, "mid": is_mid, "end": jnp.logical_not(is_mid)}
+        self.sizes = [{"all": 0, "mid": 0, "end": 0} for _ in range(send_sem.shape[0])]
+
+    def send(self, src, dst, recv_sem, device, group, kind="all", now=None):
+        def start():
+            copy = pltpu.make_async_remote_copy(
                 src_ref=src(),
                 dst_ref=dst(),
-                send_sem=self.send_sem.at[index],
+                send_sem=self.send_sem.at[group],
                 recv_sem=recv_sem(),
                 device_id=device,
                 device_id_type=MESH,
             )
-
-        self.made.append((make, cond))
-        guarded(both_of(cond, now), lambda: make().start())
-
-    def drain(self):
-        for make, cond in self.made:
-            guarded(cond, lambda make=make: make().wait_send())
+            copy.start()
+
+        self.sizes[group][kind] += size_of(src())
+        guarded(both_of(self.conds[kind], now), start)
+
+    def drain(self, spans, device):
+        for group, size in enumerate(self.sizes):
+            for kind in ("all",) if size["mid"] == size["end"] else ("mid", "end"):
+                total = size["all"] + size["mid" if kind == "all" else kind]
+
+                def wait(total=total, group=group):
+                    wait_sent(span_of(spans, total), self.send_sem.at[group], device)
+
+                guarded(self.conds[kind], wait)
+
+
+def size_of(ref):
+    return math.prod(ref.shape) * 2
+
+
+def span_of(spans, total):
+    for ref in spans:
+        count, rows, columns = ref.shape
+        need = total // (2 * columns)
+        lots = -(-need // rows)
+        if lots <= count and need % lots == 0:
+            return ref.at[pl.ds(0, lots), pl.ds(0, need // lots), :]
+    raise ValueError("no span")
+
+
+def wait_sent(ref, sem, device):
+    pltpu.make_async_remote_copy(
+        src_ref=ref, dst_ref=ref, send_sem=sem, recv_sem=sem, device_id=device, device_id_type=MESH
+    ).wait_send()
 
 
 def guarded(cond, act):
@@ -289,12 +316,6 @@
     if isinstance(start, int):
         return pl.ds(start, size)
     return pl.ds(pl.multiple_of(start, size), size)
-
-
-def send_count(n_z, chunks):
-    mixer = 4 + 10 * (n_z - 1)
-    weights = chunks + 1 + (chunks + pieces) * (2 * (n_z - 1) + 4)
-    return mixer + weights + 9
 
 
 def layer_kernel(
@@ -338,7 +359,6 @@
     chip_own,
     chip_send,
     chip_recv,
-    result,
     local_sem,
     send_sem,
     mix_sem,
@@ -352,7 +372,6 @@
     chip_recv_sem,
     out_send_sem,
     out_recv_sem,
-    write_sem,
 ):
     x = lax.axis_index("rep")
     f = lax.axis_index("fs")
@@ -373,11 +392,10 @@
     near = {1: at(other_x, z, y, t), 2: at(x, z, other_y, t), 3: at(other_x, z, other_y, t)}
     partner = at(x, z, y, other_t)
     beside = z * 2 + other_y
-    relay = n_z == 4
     toward = jnp.where(2 * z < n_z, 1, n_z - 1)
-    column = [(z + step * (toward if relay else 1)) % n_z for step in range(n_z)]
+    column = [(z + step * toward) % n_z for step in range(n_z)]
     edge = n_z - 1
-    is_mid = jnp.logical_and(z > 0, z < edge) if relay else None
+    is_mid = jnp.logical_and(z > 0, z < edge)
     mid_from = column[1:3]
     mid_to = column[edge]
     mid_device = at(x, mid_to, y, t)
@@ -386,22 +404,26 @@
         return jnp.logical_and(is_mid, z_at != mid_to)
 
     def direct(step):
-        if not relay or step == 1:
-            return None
-        return jnp.logical_not(is_mid) if step == 2 else is_mid
+        return ("all", "end", "mid")[step - 1]
+
+    barrier = pltpu.get_barrier_semaphore()
+    peers = [near[1], near[2], near[3], partner] + [at(x, w, y, t) for w in column[1:]]
+    for peer in peers:
+        pl.semaphore_signal(barrier, inc=1, device_id=peer, device_id_type=MESH)
 
     quarter = x * 2 + y
     quarter_swap = x * 2 + other_y
-    local = []
-
-    def bring(src, dst):
-        copy = pltpu.make_async_copy(src, dst, local_sem.at[len(local)])
-        copy.start()
-        local.append(copy)
-        return copy
+    numbers = itertools.count()
+
+    def bring(whole, *pairs):
+        sem = local_sem.at[next(numbers)]
+        for src, dst in pairs:
+            pltpu.make_async_copy(src, dst, sem).start()
+        return pltpu.make_async_copy(whole, whole, sem)
 
     own_rows = rows_at(f * depth, depth)
-    got_mix = [bring(mix_w, mixb.at[own_rows, :]), bring(out_w, outb.at[:, own_rows])]
+    both_blocks = mixb.at[pl.ds(0, 2 * depth), :]
+    got_mix = bring(both_blocks, (mix_w, mixb.at[own_rows, :]), (out_w, outb.at[:, own_rows]))
 
     def unit_cols(which, chunk):
         return rows_at(which * units + chunk * unit_tile, unit_tile)
@@ -410,28 +432,27 @@
     got_own, got_swap = [], []
     for c in range(chunks):
         got_own.append(
-            [
-                bring(gate_w.at[:, unit_cols(quarter, c)], gub.at[c, own_rows, low]),
-                bring(up_w.at[:, unit_cols(quarter, c)], gub.at[c, own_rows, high]),
-            ]
+            bring(
+                gub.at[c, own_rows, :],
+                (gate_w.at[:, unit_cols(quarter, c)], gub.at[c, own_rows, low]),
+                (up_w.at[:, unit_cols(quarter, c)], gub.at[c, own_rows, high]),
+            )
         )
         got_swap.append(
-            [
-                bring(gate_w.at[:, unit_cols(quarter_swap, c)], gub_swap.at[c, :, low]),
-                bring(up_w.at[:, unit_cols(quarter_swap, c)], gub_swap.at[c, :, high]),
-            ]
+            bring(
+                gub_swap.at[c],
+                (gate_w.at[:, unit_cols(quarter_swap, c)], gub_swap.at[c, :, low]),
+                (up_w.at[:, unit_cols(quarter_swap, c)], gub_swap.at[c, :, high]),
+            )
         )
-    got_tok = [bring(tokens, tok)]
-    got_own.append([bring(down_w.at[rows_at(quarter * units, units), :], dnb.at[f])])
-    got_swap.append([bring(down_w.at[rows_at(quarter_swap * units, units), :], dnb_swap)])
-
-    barrier = pltpu.get_barrier_semaphore()
-    peers = [near[1], near[2], near[3], partner] + [at(x, w, y, t) for w in column[1:]]
-    for peer in peers:
-        pl.semaphore_signal(barrier, inc=1, device_id=peer, device_id_type=MESH)
+    got_tok = bring(tok, (tokens, tok))
+    got_own.append(bring(dnb.at[f], (down_w.at[rows_at(quarter * units, units), :], dnb.at[f])))
+    got_swap.append(bring(dnb_swap, (down_w.at[rows_at(quarter_swap * units, units), :], dnb_swap)))
+
     pl.semaphore_wait(barrier, len(peers))
 
-    copies = Copies(send_sem)
+    copies = Copies(send_sem, is_mid)
+    mix_group, swap_group, down_group, act_group = range(chunks, chunks + 4)
 
     def arrived(dst, sem, cond=None):
         def wait():
@@ -453,21 +474,20 @@
         return [
             (
                 lambda: mixb.at[rows_at(block * depth + part * part_rows, part_rows), :],
-                lambda: mix_sem.at[block, 2 * part],
+                lambda: mix_sem.at[block, part],
             ),
             (
                 lambda: outb.at[rows_at(part * part_out, part_out), rows_at(block * depth, depth)],
-                lambda: mix_sem.at[block, 2 * part + 1],
+                lambda: mix_sem.at[block, part],
             ),
         ]
 
-    def send_mix(block, part, device, cond=None):
+    def send_mix(block, part, device, kind="all"):
         for ref, sem in mix_pieces(block, part):
-            copies.send(ref, ref, sem, device, cond)
+            copies.send(ref, ref, sem, device, mix_group, kind)
 
     def wait_mix(block, part):
-        for ref, sem in mix_pieces(block, part):
-            arrived(ref, sem)
+        arrived(lambda: mixb.at[rows_at(block * depth, depth), :], lambda: mix_sem.at[block, part])
 
     def weight_ref(stage, block):
         if stage == chunks:
@@ -475,28 +495,24 @@
         return lambda: gub.at[stage, rows_at(block * depth, depth), :], lambda: gu_sem.at[stage, block]
 
     def send_swap(stage):
-        for copy in got_swap[stage]:
-            copy.wait()
+        got_swap[stage].wait()
         ref, sem = weight_ref(stage, f)
-        copies.send(lambda: dnb_swap if stage == chunks else gub_swap.at[stage], ref, sem, near[2])
-
-    def send_block(stage, block, steps=range(1, n_z), also=None):
+        copies.send(lambda: dnb_swap if stage == chunks else gub_swap.at[stage], ref, sem, near[2], swap_group)
+
+    def send_block(stage, block, steps=range(1, n_z), kind=None):
         ref, sem = weight_ref(stage, block)
         for step in steps:
-            copies.send(ref, ref, sem, at(x, column[step], y, t), both_of(direct(step), also))
+            copies.send(ref, ref, sem, at(x, column[step], y, t), stage, kind or direct(step))
 
     def send_own(stage):
-        for copy in got_own[stage]:
-            copy.wait()
+        got_own[stage].wait()
         send_block(stage, f)
 
     def send_first(inner):
         if not inner:
-            for copy in got_own[0]:
-                copy.wait()
-            send_block(0, f, range(2 if relay else 1, n_z))
-        if relay:
-            send_block(0, f, range(1, 2), is_mid if inner else jnp.logical_not(is_mid))
+            got_own[0].wait()
+            send_block(0, f, range(2, n_z))
+        send_block(0, f, range(1, 2), "mid" if inner else "end")
 
     def send_beside(stage):
         arrived(*weight_ref(stage, beside))
@@ -509,44 +525,38 @@
         return lambda: dnb.at[block, :, cols], lambda: dn_sem.at[block, piece]
 
     def send_down():
-        for copy in got_own[chunks]:
-            copy.wait()
+        got_own[chunks].wait()
         arrived(*weight_ref(chunks, beside))
         for side in range(2):
             for piece in range(pieces):
                 ref, sem = down_ref(z * 2 + side, piece)
                 for step in range(1, n_z):
-                    copies.send(ref, ref, sem, at(x, column[step], y, t), direct(step))
+                    copies.send(ref, ref, sem, at(x, column[step], y, t), down_group, direct(step))
 
     side_blocks = [[z_at * 2 + side for z_at in mid_from] for side in (y, other_y)]
     mid_blocks = [[z_at * 2 + side for side in range(2)] for z_at in mid_from]
 
-    def relay_ref(ref, sem, now):
+    def relay_ref(ref, sem, group, now):
         arrived(ref, sem, both_of(is_mid, now))
-        copies.send(ref, ref, sem, mid_device, is_mid, now)
+        copies.send(ref, ref, sem, mid_device, group, "mid", now)
 
     def relay_blocks(stage, blocks, now=None):
-        if relay:
-            for block in blocks:
-                relay_ref(*weight_ref(stage, block), now)
+        for block in blocks:
+            relay_ref(*weight_ref(stage, block), stage, now)
 
     def relay_down(blocks, now=None):
-        if relay:
-            for block in blocks:
-                for piece in range(pieces):
-                    relay_ref(*down_ref(block, piece), now)
+        for block in blocks:
+            for piece in range(pieces):
+                relay_ref(*down_ref(block, piece), down_group, now)
 
     def wait_stage(stage, now=None):
         for step in range(1, n_z):
             for side in (y, other_y):
                 ref, sem = weight_ref(stage, column[step] * 2 + side)
-                fresh = None
-                if relay:
-                    fresh = jnp.logical_not(is_mid) if step < edge else None
+                fresh = jnp.logical_not(is_mid) if step < edge else None
                 arrived(ref, sem, both_of(fresh, now))
 
-    for copy in got_mix:
-        copy.wait()
+    got_mix.wait()
     for step in range(1, n_z):
         send_mix(f, x, at(x, column[step], y, t), direct(step))
     for part in range(2):
@@ -564,8 +574,7 @@
 
         lax.fori_loop(0, total // size, body, 0)
 
-    for copy in got_tok:
-        copy.wait()
+    got_tok.wait()
     norm_rows(tok, mixer_gain, acts.at[0], length)
 
     order = range(1, n_z)
@@ -574,8 +583,8 @@
         wait_mix(block, x)
         send_mix(block, x, near[2])
         send_mix(block, x, near[1])
-        if relay and step < edge:
-            send_mix(block, x, mid_device, is_mid)
+        if step < edge:
+            send_mix(block, x, mid_device, "mid")
     send_first(True)
     for stage in range(1, chunks + 1):
         send_swap(stage)
@@ -635,7 +644,7 @@
         lax.fori_loop(0, width // 512, body, 0)
 
     project(other_t, term_send)
-    copies.send(lambda: term_send, lambda: term_recv, lambda: term_sem.at[0], partner)
+    copies.send(lambda: term_send, lambda: term_recv, lambda: term_sem.at[0], partner, act_group)
     project(t, term_own)
     arrived(lambda: term_recv, lambda: term_sem.at[0])
     mine = rows_at(t * half, half)
@@ -657,8 +666,8 @@
         return lambda: act_sem.at[slot, hop]
 
     for slot in (1, 2, 3):
-        copies.send(act_part(0, mine), act_part(slot, mine), act_arrival(slot, 0), near[slot])
-    copies.send(act_part(0, mine), act_part(0, mine), act_arrival(0, 1), partner)
+        copies.send(act_part(0, mine), act_part(slot, mine), act_arrival(slot, 0), near[slot], act_group)
+    copies.send(act_part(0, mine), act_part(0, mine), act_arrival(0, 1), partner, act_group)
     relay_blocks(1, side_blocks[1])
     relay_blocks(2, side_blocks[0])
     relay_blocks(2, side_blocks[1])
@@ -666,7 +675,7 @@
 
     def pass_on(slot, now):
         arrived(act_part(slot, mine), act_arrival(slot, 0), now)
-        copies.send(act_part(slot, mine), act_part(slot, mine), act_arrival(slot, 1), partner, None, now)
+        copies.send(act_part(slot, mine), act_part(slot, mine), act_arrival(slot, 1), partner, act_group, now=now)
 
     def wait_acts(slot, now):
         arrived(act_part(slot, theirs), act_arrival(slot, 1), now)
@@ -716,9 +725,7 @@
 
     def block_of(i):
         k, side = i // (2 * pieces), (i // pieces) % 2
-        if n_z == 4:
-            return (((z // 2 + k // 2) % 2) * 2 + (z % 2 + k % 2) % 2) * 2 + side
-        return ((z + k) % n_z) * 2 + side
+        return (((z // 2 + k // 2) % 2) * 2 + (z % 2 + k % 2) % 2) * 2 + side
 
     def cols_of(i):
         return rows_at((block_of(i) * pieces + i % pieces) * piece_width, piece_width)
@@ -745,7 +752,7 @@
 
     def out_copy(i):
         return pltpu.make_async_remote_copy(
-            src_ref=result.at[:, cols_of(i)],
+            src_ref=out.at[mine, cols_of(i)],
             dst_ref=out.at[mine, cols_of(i)],
             send_sem=out_send_sem.at[0],
             recv_sem=out_recv_sem.at[0],
@@ -753,9 +760,6 @@
             device_id_type=MESH,
         )
 
-    def write_copy(i):
-        return pltpu.make_async_copy(result.at[:, cols_of(i)], out.at[mine, cols_of(i)], write_sem.at[0])
-
     lag = 3
 
     def down_body(i, carry):
@@ -763,8 +767,7 @@
 
         block, cols = block_of(i), rows_at((i % pieces) * piece_width, piece_width)
         fresh = jnp.logical_and(block != f, block != beside)
-        if relay:
-            fresh = jnp.logical_and(fresh, jnp.logical_not(relayed(block // 2)))
+        fresh = jnp.logical_and(fresh, jnp.logical_not(relayed(block // 2)))
         arrived(lambda: dnb.at[block, :, cols], lambda: dn_sem.at[block, i % pieces], fresh)
         weight = dnb[block, :, cols]
         half_send[i] = jnp.dot(hid[other_t], weight, preferred_element_type=jnp.float32).astype(jnp.bfloat16)
@@ -793,27 +796,20 @@
         total = chip_own[m]
         for slot in range(3):
             total = total + chip_recv[m, slot].astype(jnp.float32)
-        result[:, cols_of(m)] = (residual[:, cols_of(m)].astype(jnp.float32) + total).astype(jnp.bfloat16)
+        out[mine, cols_of(m)] = (residual[:, cols_of(m)].astype(jnp.float32) + total).astype(jnp.bfloat16)
         out_copy(m).start()
-        write_copy(m).start()
 
     def finish_body(m, carry):
         finish(m)
         return carry
 
     lax.fori_loop(0, n_b, down_body, 0)
-    copies.drain()
+    copies.drain((gub, acts), partner)
     lax.fori_loop(n_b - lag, n_b, finish_body, 0)
 
-    def sent(ref, sem):
-        pltpu.make_async_remote_copy(
-            src_ref=ref, dst_ref=ref, send_sem=sem, recv_sem=sem, device_id=partner, device_id_type=MESH
-        ).wait_send()
-
-    sent(half_send, half_send_sem.at[0])
-    sent(chip_send, chip_send_sem.at[0])
-    sent(result, out_send_sem.at[0])
-    pltpu.make_async_copy(result, out.at[mine, :], write_sem.at[0]).wait()
+    wait_sent(half_send, half_send_sem.at[0], partner)
+    wait_sent(chip_send, chip_send_sem.at[0], partner)
+    wait_sent(out.at[mine, :], out_send_sem.at[0], partner)
     arrived(lambda: out.at[theirs, :], lambda: out_recv_sem.at[0])
 
 
@@ -891,8 +887,8 @@
         functools.partial(layer_kernel, n_z),
         name="layer",
         in_specs=[hbm, vmem, hbm] + [vmem] * 7 + [hbm, vmem, hbm, hbm, vmem, vmem, hbm],
-        out_specs=hbm,
-        out_shape=jax.ShapeDtypeStruct((length, width), bf16),
+        out_specs=vmem,
+        out_shape=pltpu.VMEM((length, width), bf16),
         scratch_shapes=[
             pltpu.VMEM((length, width), bf16),
             pltpu.VMEM((width, channels), bf16),
@@ -915,10 +911,9 @@
             pltpu.VMEM((n_b, half, depth // pieces), f32),
             pltpu.VMEM((n_b, 3, half, depth // pieces), bf16),
             pltpu.VMEM((n_b, 3, half, depth // pieces), bf16),
-            pltpu.VMEM((half, width), bf16),
-            dma((5 + 4 * chunks,)),
-            dma((send_count(n_z, chunks),)),
-            dma((n_fs, 4)),
+            dma((4 + 2 * chunks,)),
+            dma((chunks + 4,)),
+            dma((n_fs, 2)),
             dma((chunks, n_fs)),
             dma((n_fs, pieces)),
             dma((1,)),
@@ -927,7 +922,6 @@
             dma((n_b,)),
             dma((1,)),
             dma((n_b,)),
-            dma((1,)),
             dma((1,)),
             dma((1,)),
         ],
@@ -953,38 +947,12 @@
         row(gate_offset),
         down_weight,
     )
-    parts = 4
-    return pl.pallas_call(
-        write_out,
-        name="write_out",
-        in_specs=[pl.BlockSpec(memory_space=pltpu.HBM)],
-        out_specs=pl.BlockSpec(memory_space=pltpu.HBM),
-        out_shape=jax.ShapeDtypeStruct((length, width), bf16),
-        scratch_shapes=[pltpu.VMEM((parts, length // parts, width), bf16), dma((2, parts))],
-        compiler_params=pltpu.CompilerParams(vmem_limit_bytes=62 * 2**20),
-    )(rows_out)
-
-
-def write_out(rows_ref, out_ref, held, sem):
-    parts, size, _ = held.shape
-    copies_in = [
-        pltpu.make_async_copy(rows_ref.at[pl.ds(k * size, size), :], held.at[k], sem.at[0, k]) for k in range(parts)
-    ]
-    copies_out = [
-        pltpu.make_async_copy(held.at[k], out_ref.at[pl.ds(k * size, size), :], sem.at[1, k]) for k in range(parts)
-    ]
-    for copy in copies_in:
-        copy.start()
-    for k in range(parts):
-        copies_in[k].wait()
-        copies_out[k].start()
-    for copy in copies_out:
-        copy.wait()
+    return rows_out
 
 
 def local(n_rep, n_fs, n_tp, *arrays):
     units, columns = arrays[16].shape
-    fits = n_rep == 2 and n_tp == 2 and n_fs % 2 == 0 and n_fs <= 8
+    fits = n_rep == 2 and n_tp == 2 and n_fs == 8
     if fits and units == 12 * unit_tile and columns % 128 == 0:
         return fused(n_fs, *arrays)
     return plain(n_rep, n_fs, n_tp, *arrays)

time: 189 us -> 187 us (0.989)
  Pallas kernels: 189 us -> 185 us
    pallas_call x1 -> x0, Pallas kernels: 2.42 us -> none  [fused(): pl.pallas_call(write_out, name='write_out', in_specs=[pl.BlockSpec(memory...]
where the time goes in v3:
time: 187 us
  Pallas kernels  185 us (99%)
    pallas_call x1, Pallas kernels, fused(): pl.pallas_call(functools.partial(layer_kernel, n_z), name='layer', in_spe...  185 us

profile of v3, /device:TPU:0, one launch (start us, length us, event | category | flops | bytes accessed | tf_op | source)
XLA Modules:
  0.0 186.7 jit_solution(11762425974589482685)
XLA Ops:
  0.0 185.3 %layer.1 = bf16[512,2048]{1,0:T(8,128)(2,1)S(1)} custom-call(bf16[512,2048]{1,0:T(8,128)(2,1)} %tokens.1, f32[1,2048]{1,0:T(1,128)} %bitcast.8, bf16[256,512]{1,0:T(8,128)(2,1)} %mix_w.1, f32[4,512]{1,0:T(4,128)} %taps.1, f32[1,512]{1,0:T(1,128)} %bitcast.10, bf16[4,128,128]{2,1,0:T(8,128)(2,1)} %recur_w.1, f32[1,512]{1,0:T(1,128)} %bitcast.11, ...), custom_call_target="tpu_custom_call" | custom-call | tf_op jit(solution)/shard_map/layer/pallas_call | solution.py:886
  185.3 1.3 copy.19

commit v4 on v3

--- a/solution.py
+++ b/solution.py
@@ -407,9 +407,15 @@
         return ("all", "end", "mid")[step - 1]
 
     barrier = pltpu.get_barrier_semaphore()
-    peers = [near[1], near[2], near[3], partner] + [at(x, w, y, t) for w in column[1:]]
-    for peer in peers:
+
+    def greet(peer):
         pl.semaphore_signal(barrier, inc=1, device_id=peer, device_id_type=MESH)
+
+    beside_peers = [near[1], near[2], near[3], partner]
+    for peer in [at(x, column[1], y, t)] + beside_peers:
+        greet(peer)
+    for step in range(2, n_z):
+        guarded(is_mid, functools.partial(greet, at(x, column[step], y, t)))
 
     quarter = x * 2 + y
     quarter_swap = x * 2 + other_y
@@ -449,7 +455,7 @@
     got_own.append(bring(dnb.at[f], (down_w.at[rows_at(quarter * units, units), :], dnb.at[f])))
     got_swap.append(bring(dnb_swap, (down_w.at[rows_at(quarter_swap * units, units), :], dnb_swap)))
 
-    pl.semaphore_wait(barrier, len(peers))
+    pl.semaphore_wait(barrier, len(beside_peers) + 2)
 
     copies = Copies(send_sem, is_mid)
     mix_group, swap_group, down_group, act_group = range(chunks, chunks + 4)

time: 187 us -> 186 us (level)
  no operation moved by 1% of the time
where the time goes in v4:
time: 186 us
  Pallas kernels  184 us (99%)
    pallas_call x1, Pallas kernels, fused(): pl.pallas_call(functools.partial(layer_kernel, n_z), name='layer', in_spe...  184 us

profile of v4, /device:TPU:0, one launch (start us, length us, event | category | flops | bytes accessed | tf_op | source)
XLA Modules:
  0.0 185.6 jit_solution(17323072006725291387)
XLA Ops:
  0.0 184.3 %layer.1 = bf16[512,2048]{1,0:T(8,128)(2,1)S(1)} custom-call(bf16[512,2048]{1,0:T(8,128)(2,1)} %tokens.1, f32[1,2048]{1,0:T(1,128)} %bitcast.8, bf16[256,512]{1,0:T(8,128)(2,1)} %mix_w.1, f32[4,512]{1,0:T(4,128)} %taps.1, f32[1,512]{1,0:T(1,128)} %bitcast.10, bf16[4,128,128]{2,1,0:T(8,128)(2,1)} %recur_w.1, f32[1,512]{1,0:T(1,128)} %bitcast.11, ...), custom_call_target="tpu_custom_call" | custom-call | tf_op jit(solution)/shard_map/layer/pallas_call | solution.py:892
  184.3 1.3 copy.19
